TPU v7x, 32 devices: a whole 2x2x4 slice. The times are simulated.
32 devices in a mesh: ep: 8 (over z, core), tp: 4 (over y, x).
Axes of the slice: x: 2, y: 2, z: 4, core: 2. Of those that a mesh axis runs over, the one named last changes fastest.
Arguments:
- tokens: bfloat16 [1536, 4096], P('ep'), may hold values from -6 to 6
- expert_ids: int32 [1536, 2], P('ep'), may hold values from 0 to 7, all different within a row; in each aligned block of 192 rows (0 to 191, 192 to 383, ...) at most 60 rows name the same one
- route_weight: float32 [1536, 2], P('ep'), may hold values from 0.1 to 1
- norm_gain: float32 [4096], replicated, may hold values from 0.1 to 1.9
- gate_weight: bfloat16 [8, 4096, 4096], P('ep', None, 'tp'), may hold values from -0.28125 to 0.28125
- up_weight: bfloat16 [8, 4096, 4096], P('ep', None, 'tp'), may hold values from -0.28125 to 0.28125
- down_weight: bfloat16 [8, 4096, 4096], P('ep', None, 'tp'), may hold values from -0.028076172 to 0.028076172
Outputs:
- mixed: bfloat16 [1536, 4096], P('ep', 'tp')
Inputs may be any that keep to these rules, and one draw needn't show every extreme that they name: `expert_ids`: each row names 2 different experts. In each aligned block of 192 rows (the tokens of one index of ep) no expert is named by more than 60 rows, and in some block some expert is named by exactly 60 rows.
All inputs are finite; a program needn't handle non-finite values.
Results may differ from a plain program's by a relative error of at most 0.007.
Values may be sent and summed in bfloat16 or wider, within the bound.
A program may use at most 64 MiB of HBM per device.

v0:
```python
import functools

import jax
import jax.numpy as jnp
from jax import lax
from jax.experimental import pallas as pl
from jax.experimental.pallas import tpu as pltpu
from jax.sharding import PartitionSpec as P

EPS = 1e-06
LIMIT = 7.0
ALPHA = 1.702


def rms_norm(tokens, norm_gain):
    values = tokens.astype(jnp.float32)
    scale = lax.rsqrt(jnp.mean(values * values, axis=-1, keepdims=True) + EPS)
    return (values * scale * norm_gain).astype(jnp.bfloat16)


def clamped_unit(gate_pre, up_pre):
    gate = jnp.minimum(gate_pre, LIMIT)
    up_part = jnp.clip(up_pre, -LIMIT, LIMIT)
    return ((up_part + 1.0) * gate * jax.nn.sigmoid(ALPHA * gate)).astype(jnp.bfloat16)


def slot_numbers(id_blocks, experts, capacity):
    onehot = (id_blocks[:, :, None] == jnp.arange(experts, dtype=jnp.int32)[None, None, :]).astype(
        jnp.int32
    )
    before = jnp.cumsum(onehot, axis=1) - onehot
    position = jnp.sum(before * onehot, axis=2)
    return id_blocks * capacity + position


def project_down(hidden, down_weight):
    result = jnp.einsum(
        "sejf,efd->sejd",
        lax.all_gather(hidden, "tp", axis=3, tiled=True),
        down_weight,
        preferred_element_type=jnp.float32,
    )
    return result.astype(jnp.bfloat16)


def plain_path(tokens, expert_ids, route_weight, norm_gain, gate_weight, up_weight, down_weight):
    n_ep = lax.axis_size("ep")
    n_tp = lax.axis_size("tp")
    tok_rows, width = tokens.shape
    top = expert_ids.shape[1]
    local_experts = gate_weight.shape[0]
    experts = local_experts * n_ep
    capacity = 5 * tok_rows * top // (4 * experts)
    cols = width // n_tp
    normed = rms_norm(tokens, norm_gain)
    dest = slot_numbers(expert_ids.reshape(1, tok_rows * top), experts, capacity).reshape(-1)
    slot_range = jnp.arange(experts * capacity, dtype=jnp.int32)
    match = slot_range[:, None] == dest[None, :]
    pick = jnp.any(match.reshape(experts * capacity, tok_rows, top), axis=2).astype(jnp.bfloat16)
    own = lax.dynamic_slice_in_dim(normed, lax.axis_index("tp") * cols, cols, 1)
    buffer = jnp.dot(pick, own, preferred_element_type=jnp.float32).astype(jnp.bfloat16)
    buffer = buffer.reshape(n_ep, local_experts, capacity, cols)
    arrived = lax.all_to_all(buffer, "ep", split_axis=0, concat_axis=0, tiled=True)
    piece = lax.all_gather(arrived, "tp", axis=3, tiled=True)
    gate_part = jnp.einsum("sejd,edf->sejf", piece, gate_weight, preferred_element_type=jnp.float32)
    up_part = jnp.einsum("sejd,edf->sejf", piece, up_weight, preferred_element_type=jnp.float32)
    hidden = clamped_unit(gate_part, up_part)
    result = project_down(hidden, down_weight)
    back = lax.all_to_all(result, "ep", split_axis=0, concat_axis=0, tiled=True).reshape(
        experts * capacity, cols
    )
    chosen = jnp.transpose(match).astype(jnp.bfloat16)
    per_copy = jnp.dot(chosen, back, preferred_element_type=jnp.float32).reshape(
        tok_rows, top, cols
    )
    mixed = jnp.sum(per_copy * route_weight[:, :, None], axis=1)
    return mixed.astype(jnp.bfloat16)


VMEM_BYTES = 46 * 1024 * 1024
COLUMN_TILE = 256


def flip(value, bits):
    bit = 1
    while bit <= bits:
        if bits & bit:
            value = value + bit - 2 * bit * lax.rem(lax.div(value, jnp.int32(bit)), jnp.int32(2))
        bit *= 2
    return value


def fused_kernel(
    n_ep,
    n_tp,
    slots,
    tokens_hbm,
    ids_row_hbm,
    route_row_hbm,
    gain_hbm,
    gate_hbm,
    up_hbm,
    down_hbm,
    out_ref,
    tokens_ref,
    ids_row_ref,
    route_row_ref,
    gain_ref,
    gate_v,
    up_v,
    down_v,
    scales,
    normed,
    outbox,
    fullbox,
    xbuf,
    hbuf,
    obuf,
    back,
    small_sem,
    weight_sem,
    z_send,
    z_recv,
    pair_send,
    pair_recv,
    g_send,
    g_recv,
    b_send,
    b_recv,
):
    pairs = n_ep // 2
    tok_rows = tokens_ref.shape[0]
    cols = xbuf.shape[-1]
    hid = hbuf.shape[-1]
    outs = obuf.shape[-1]
    ep = lax.axis_index("ep")
    tp = lax.axis_index("tp")
    pair = lax.div(ep, jnp.int32(2))
    core = lax.rem(ep, jnp.int32(2))
    side = (flip(tp, 1), flip(tp, 2))
    far = flip(tp, 3)

    small = (
        (tokens_hbm, tokens_ref),
        (ids_row_hbm, ids_row_ref),
        (route_row_hbm, route_row_ref),
        (gain_hbm, gain_ref),
    )
    small_loads = [
        pltpu.make_async_copy(a, b, small_sem.at[i]) for i, (a, b) in enumerate(small)
    ]
    for load in small_loads:
        load.start()
    loads = [
        pltpu.make_async_copy(hbm.at[0], vmem, weight_sem.at[i])
        for i, (hbm, vmem) in enumerate(((gate_hbm, gate_v), (up_hbm, up_v), (down_hbm, down_v)))
    ]
    for load in loads:
        load.start()

    barrier = pltpu.get_barrier_semaphore()
    for k in range(1, n_ep):
        pl.semaphore_signal(
            barrier, inc=1, device_id=(flip(ep, k), tp), device_id_type=pl.DeviceIdType.MESH
        )
    for other in side:
        pl.semaphore_signal(
            barrier, inc=1, device_id=(ep, other), device_id_type=pl.DeviceIdType.MESH
        )

    for load in small_loads:
        load.wait()

    own_cols = pl.ds(pl.multiple_of(tp * cols, cols), cols)

    def scale_rows(i, carry):
        rows = pl.ds(pl.multiple_of(i * 16, 16), 16)
        values = tokens_ref[rows, :].astype(jnp.float32)
        scale = lax.rsqrt(jnp.mean(values * values, axis=-1, keepdims=True) + EPS)
        scales[rows, :] = jnp.broadcast_to(scale, (16, scales.shape[1]))
        values = tokens_ref[rows, own_cols].astype(jnp.float32)
        normed[rows, own_cols] = (values * scale * gain_ref[:, own_cols]).astype(jnp.bfloat16)
        return carry

    lax.fori_loop(0, tok_rows // 16, scale_rows, 0)

    ids_row = ids_row_ref[...]
    expert_col = lax.broadcasted_iota(jnp.int32, (n_ep, tok_rows), 0)
    hits_row = ((ids_row[0:1, :] == expert_col) | (ids_row[1:2, :] == expert_col)).astype(
        jnp.float32
    ).astype(jnp.bfloat16)
    first = lax.broadcasted_iota(jnp.int32, (tok_rows, tok_rows), 0)
    second = lax.broadcasted_iota(jnp.int32, (tok_rows, tok_rows), 1)
    earlier = (first < second).astype(jnp.float32).astype(jnp.bfloat16)
    before_row = jnp.dot(hits_row, earlier, preferred_element_type=jnp.float32)
    slot_row = [
        jnp.sum(jnp.where(ids_row[k : k + 1, :] == expert_col, before_row, 0.0), axis=0, keepdims=True)
        for k in range(2)
    ]
    slot_at = lax.broadcasted_iota(jnp.int32, (slots, tok_rows), 0).astype(jnp.float32)

    def pick_of(expert):
        taken = ((ids_row[0:1, :] == expert) & (slot_row[0] == slot_at)) | (
            (ids_row[1:2, :] == expert) & (slot_row[1] == slot_at)
        )
        return taken.astype(jnp.float32).astype(jnp.bfloat16)

    pl.semaphore_wait(barrier, n_ep - 1 + 2)

    def z_copy(k, c):
        return pltpu.make_async_remote_copy(
            src_ref=outbox.at[k - 1, c],
            dst_ref=xbuf.at[k, tp, core],
            send_sem=z_send.at[k, c],
            recv_sem=z_recv.at[k, core],
            device_id=(flip(pair, k) * 2 + c, tp),
            device_id_type=pl.DeviceIdType.MESH,
        )

    def z_arrival(k, c):
        return pltpu.make_async_remote_copy(
            src_ref=outbox.at[k - 1, c],
            dst_ref=xbuf.at[k, tp, c],
            send_sem=z_send.at[k, c],
            recv_sem=z_recv.at[k, c],
            device_id=(flip(pair, k) * 2 + c, tp),
            device_id_type=pl.DeviceIdType.MESH,
        )

    for k in range(1, pairs):
        for c in range(2):
            outbox[k - 1, c] = jnp.dot(
                pick_of(flip(pair, k) * 2 + c),
                normed[:, own_cols],
                preferred_element_type=jnp.float32,
            ).astype(jnp.bfloat16)
            z_copy(k, c).start()

    def norm_rows(i, carry):
        rows = pl.ds(pl.multiple_of(i * 16, 16), 16)
        values = tokens_ref[rows, :].astype(jnp.float32)
        normed[rows, :] = (values * scales[rows, 0:1] * gain_ref[...]).astype(jnp.bfloat16)
        return carry

    lax.fori_loop(0, tok_rows // 16, norm_rows, 0)

    partner = flip(ep, 1)
    pair_copy = pltpu.make_async_remote_copy(
        src_ref=fullbox,
        dst_ref=xbuf.at[0, :, core],
        send_sem=pair_send,
        recv_sem=pair_recv,
        device_id=(partner, tp),
        device_id_type=pl.DeviceIdType.MESH,
    )
    pair_arrival = pltpu.make_async_remote_copy(
        src_ref=fullbox,
        dst_ref=xbuf.at[0, :, 1 - core],
        send_sem=pair_send,
        recv_sem=pair_recv,
        device_id=(partner, tp),
        device_id_type=pl.DeviceIdType.MESH,
    )
    theirs = pick_of(partner)
    for j in range(n_tp):
        fullbox[j] = jnp.dot(
            theirs, normed[:, j * cols : (j + 1) * cols], preferred_element_type=jnp.float32
        ).astype(jnp.bfloat16)
    pair_copy.start()
    mine = pick_of(ep)
    for j in range(n_tp):
        xbuf[0, j, core] = jnp.dot(
            mine, normed[:, j * cols : (j + 1) * cols], preferred_element_type=jnp.float32
        ).astype(jnp.bfloat16)

    boxes = (xbuf, hbuf)

    def block_copy(b, k, d, half):
        return pltpu.make_async_remote_copy(
            src_ref=boxes[b].at[k, tp, half],
            dst_ref=boxes[b].at[k, tp, half],
            send_sem=g_send.at[b, k, 2 * d + half],
            recv_sem=g_recv.at[b, k, 2 * d + half],
            device_id=(ep, side[d]),
            device_id_type=pl.DeviceIdType.MESH,
        )

    def block_arrival(b, k, d, half):
        return pltpu.make_async_remote_copy(
            src_ref=boxes[b].at[k, side[d], half],
            dst_ref=boxes[b].at[k, side[d], half],
            send_sem=g_send.at[b, k, 2 * d + half],
            recv_sem=g_recv.at[b, k, 2 * d + half],
            device_id=(ep, side[d]),
            device_id_type=pl.DeviceIdType.MESH,
        )

    def relay_copy(b, k, d):
        return pltpu.make_async_remote_copy(
            src_ref=boxes[b].at[k, side[d], d],
            dst_ref=boxes[b].at[k, side[d], d],
            send_sem=g_send.at[b, k, 4 + d],
            recv_sem=g_recv.at[b, k, 4 + d],
            device_id=(ep, side[1 - d]),
            device_id_type=pl.DeviceIdType.MESH,
        )

    def relay_arrival(b, k, d):
        return pltpu.make_async_remote_copy(
            src_ref=boxes[b].at[k, far, d],
            dst_ref=boxes[b].at[k, far, d],
            send_sem=g_send.at[b, k, 4 + d],
            recv_sem=g_recv.at[b, k, 4 + d],
            device_id=(ep, side[1 - d]),
            device_id_type=pl.DeviceIdType.MESH,
        )

    def spread(b, k):
        for step in range(2):
            for d in range(2):
                block_copy(b, k, d, d if step == 0 else 1 - d).start()

    def relay(b, k):
        for d in range(2):
            block_arrival(b, k, d, d).wait_recv()
            relay_copy(b, k, d).start()

    def gathered(b, k):
        for d in range(2):
            block_arrival(b, k, d, 1 - d).wait_recv()
        for d in range(2):
            relay_arrival(b, k, d).wait_recv()

    def enter(k):
        for c in range(2):
            z_arrival(k, c).wait_recv()
        spread(0, k)

    def dot_blocks(box, k, weight, where):
        depth = box.shape[-1]
        total = None
        for j in range(n_tp):
            part = jnp.dot(
                box[k, j].reshape(2 * slots, depth),
                weight[j * depth : (j + 1) * depth, where],
                preferred_element_type=jnp.float32,
            )
            total = part if total is None else total + part
        return total

    def units(k):
        def tile(i, carry):
            where = pl.ds(pl.multiple_of(i * COLUMN_TILE, COLUMN_TILE), COLUMN_TILE)
            gate_pre = dot_blocks(xbuf, k, gate_v, where)
            up_pre = dot_blocks(xbuf, k, up_v, where)
            hidden = clamped_unit(gate_pre, up_pre)
            hbuf[k, tp, :, :, where] = hidden.reshape(2, slots, COLUMN_TILE)
            return carry

        lax.fori_loop(0, hid // COLUMN_TILE, tile, 0)

    def back_copy(k, c):
        return pltpu.make_async_remote_copy(
            src_ref=obuf.at[k, c],
            dst_ref=back.at[ep],
            send_sem=b_send.at[k, c],
            recv_sem=b_recv.at[ep],
            device_id=(flip(pair, k) * 2 + c, tp),
            device_id_type=pl.DeviceIdType.MESH,
        )

    def back_arrival(flips):
        other = flip(ep, flips)
        return pltpu.make_async_remote_copy(
            src_ref=obuf.at[0, 0],
            dst_ref=back.at[other],
            send_sem=b_send.at[0, 0],
            recv_sem=b_recv.at[other],
            device_id=(other, tp),
            device_id_type=pl.DeviceIdType.MESH,
        )

    partner_back = pltpu.make_async_remote_copy(
        src_ref=obuf.at[0, 1 - core],
        dst_ref=back.at[ep],
        send_sem=b_send.at[0, 0],
        recv_sem=b_recv.at[ep],
        device_id=(partner, tp),
        device_id_type=pl.DeviceIdType.MESH,
    )

    def results(k):
        def tile(i, carry):
            where = pl.ds(pl.multiple_of(i * COLUMN_TILE, COLUMN_TILE), COLUMN_TILE)
            total = dot_blocks(hbuf, k, down_v, where).astype(jnp.bfloat16)
            obuf[k, :, :, where] = total.reshape(2, slots, COLUMN_TILE)
            return carry

        lax.fori_loop(0, outs // COLUMN_TILE, tile, 0)
        if k == 0:
            partner_back.start()
            back[ep] = obuf[0, core]
        else:
            for c in range(2):
                back_copy(k, c).start()

    loads[0].wait()
    loads[1].wait()
    pair_arrival.wait_recv()
    units(0)
    enter(1)
    relay(0, 1)
    if pairs > 2:
        enter(2)
    loads[2].wait()
    for k in range(1, pairs):
        gathered(0, k)
        units(k)
        spread(1, k)
        if k + 1 < pairs:
            relay(0, k + 1)
        if k + 2 < pairs:
            enter(k + 2)
        if k == pairs - 1:
            spread(1, 0)
        if k >= 2:
            gathered(1, k - 1)
            results(k - 1)
        relay(1, k)
    gathered(1, pairs - 1)
    results(pairs - 1)
    relay(1, 0)
    gathered(1, 0)
    results(0)

    place = lax.broadcasted_iota(jnp.int32, (n_ep * slots, tok_rows), 0).astype(jnp.float32)
    share = None
    for k in range(2):
        spot = ids_row[k : k + 1, :].astype(jnp.float32) * slots + slot_row[k]
        part = jnp.where(place == spot, route_row_ref[k : k + 1, :], 0.0)
        share = part if share is None else share + part
    share = jnp.transpose(share)
    share_high = share.astype(jnp.bfloat16)
    share_low = (share - share_high.astype(jnp.float32)).astype(jnp.bfloat16)

    for flips in range(1, n_ep):
        back_arrival(flips).wait_recv()

    def mix(i, carry):
        where = pl.ds(pl.multiple_of(i * COLUMN_TILE, COLUMN_TILE), COLUMN_TILE)
        table = back[:, :, where].reshape(n_ep * slots, COLUMN_TILE)
        total = jnp.dot(share_high, table, preferred_element_type=jnp.float32)
        total = total + jnp.dot(share_low, table, preferred_element_type=jnp.float32)
        out_ref[:, where] = total.astype(jnp.bfloat16)
        return carry

    lax.fori_loop(0, outs // COLUMN_TILE, mix, 0)

    for k in range(1, pairs):
        for c in range(2):
            z_copy(k, c).wait_send()
            back_copy(k, c).wait_send()
    pair_copy.wait_send()
    partner_back.wait_send()
    for k in range(pairs):
        for b in range(2):
            if b == 0 and k == 0:
                continue
            for d in range(2):
                for half in range(2):
                    block_copy(b, k, d, half).wait_send()
                relay_copy(b, k, d).wait_send()


def fused_path(
    n_ep, n_tp, tokens, expert_ids, route_weight, norm_gain, gate_weight, up_weight, down_weight
):
    tok_rows, width = tokens.shape
    slots = slots_of(n_ep, tokens.shape, expert_ids.shape)
    hid = gate_weight.shape[2]
    outs = down_weight.shape[2]
    cols = width // n_tp
    pairs = n_ep // 2
    vmem = pl.BlockSpec(memory_space=pltpu.VMEM)
    hbm = pl.BlockSpec(memory_space=pltpu.HBM)
    dma = pltpu.SemaphoreType.DMA
    arrays = (
        tokens,
        jnp.transpose(expert_ids),
        jnp.transpose(route_weight),
        norm_gain.reshape(1, width),
        gate_weight,
        up_weight,
        down_weight,
    )
    return pl.pallas_call(
        functools.partial(fused_kernel, n_ep, n_tp, slots),
        out_shape=jax.ShapeDtypeStruct((tok_rows, outs), jnp.bfloat16),
        in_specs=[hbm] * 7,
        out_specs=vmem,
        scratch_shapes=[
            pltpu.VMEM(tokens.shape, tokens.dtype),
            pltpu.VMEM(expert_ids.shape[::-1], expert_ids.dtype),
            pltpu.VMEM(route_weight.shape[::-1], route_weight.dtype),
            pltpu.VMEM((1, width), norm_gain.dtype),
            pltpu.VMEM(gate_weight.shape[1:], jnp.bfloat16),
            pltpu.VMEM(up_weight.shape[1:], jnp.bfloat16),
            pltpu.VMEM(down_weight.shape[1:], jnp.bfloat16),
            pltpu.VMEM((tok_rows, 128), jnp.float32),
            pltpu.VMEM((tok_rows, width), jnp.bfloat16),
            pltpu.VMEM((pairs - 1, 2, slots, cols), jnp.bfloat16),
            pltpu.VMEM((n_tp, slots, cols), jnp.bfloat16),
            pltpu.VMEM((pairs, n_tp, 2, slots, cols), jnp.bfloat16),
            pltpu.VMEM((pairs, n_tp, 2, slots, hid), jnp.bfloat16),
            pltpu.VMEM((pairs, 2, slots, outs), jnp.bfloat16),
            pltpu.VMEM((n_ep, slots, outs), jnp.bfloat16),
            dma((4,)),
            dma((3,)),
            dma((pairs, 2)),
            dma((pairs, 2)),
            dma,
            dma,
            dma((2, pairs, 6)),
            dma((2, pairs, 6)),
            dma((pairs, 2)),
            dma((n_ep,)),
        ],
        compiler_params=pltpu.CompilerParams(
            collective_id=0, has_side_effects=True, vmem_limit_bytes=VMEM_BYTES
        ),
    )(*(pltpu.with_memory_space_constraint(array, pltpu.HBM) for array in arrays))


def slots_of(n_ep, token_shape, id_shape):
    capacity = 5 * token_shape[0] * id_shape[1] // (4 * n_ep)
    return -(-capacity // 16) * 16


def on_device(tokens, expert_ids, route_weight, norm_gain, gate_weight, up_weight, down_weight):
    n_ep = lax.axis_size("ep")
    n_tp = lax.axis_size("tp")
    args = (tokens, expert_ids, route_weight, norm_gain, gate_weight, up_weight, down_weight)
    fits = n_tp == 4 and n_ep >= 4 and n_ep & (n_ep - 1) == 0 and gate_weight.shape[0] == 1
    if fits and expert_ids.shape[1] == 2:
        return fused_path(n_ep, n_tp, *args)
    return plain_path(*args)


def solution(mesh):
    placed = (
        P("ep", None),
        P("ep", None),
        P("ep", None),
        P(),
        P("ep", None, "tp"),
        P("ep", None, "tp"),
        P("ep", None, "tp"),
    )
    return jax.shard_map(
        on_device, mesh=mesh, in_specs=placed, out_specs=P("ep", "tp"), check_vma=False
    )
```

profile of v0, /device:TPU:1, one launch (start us, length us, event | category | flops | bytes accessed | tf_op | source)
XLA Modules:
  0.0 93.0 jit_solution(223502599656467812)
XLA Ops:
  0.0 92.3 %shard_map.73 = bf16[192,1024]{1,0:T(8,128)(2,1)S(1)} custom-call(bf16[192,4096]{1,0:T(8,128)(2,1)} %tokens_hbm.1, s32[2,192]{1,0:T(2,128)} %bitcast.4, f32[2,192]{1,0:T(2,128)} %bitcast.5, f32[1,4096]{1,0:T(1,128)} %bitcast.3, bf16[1,4096,1024]{2,1,0:T(8,128)(2,1)} %gate_hbm.1, bf16[1,4096,1024]{2,1,0:T(8,128)(2,1)} %up_hbm.1, bf16[1,4096,1024]{2,1,0:T(8,128)(2,1)} %down_hbm.1), custom_call_target="tpu_custom_call" | custom-call | tf_op jit(solution)/shard_map/pallas_call | solution.py:496
  92.3 0.7 copy.9
where the time goes:
time: 94.3 us; the launch traced here: 93 us
  Pallas kernels  92.3 us (98%)
    pallas_call x1, Pallas kernels, fused_path(): pl.pallas_call(functools.partial(fused_kernel, n_ep, n_tp, slots), out_sh...  92.3 us

commit v1 on v0

v1 whole, which is shorter than its diff:
```python
import functools

import jax
import jax.numpy as jnp
from jax import lax
from jax.experimental import pallas as pl
from jax.experimental.pallas import tpu as pltpu
from jax.sharding import PartitionSpec as P

EPS = 1e-06
LIMIT = 7.0
ALPHA = 1.702


def rms_norm(tokens, norm_gain):
    values = tokens.astype(jnp.float32)
    scale = lax.rsqrt(jnp.mean(values * values, axis=-1, keepdims=True) + EPS)
    return (values * scale * norm_gain).astype(jnp.bfloat16)


def clamped_unit(gate_pre, up_pre):
    gate = jnp.minimum(gate_pre, LIMIT)
    up_part = jnp.clip(up_pre, -LIMIT, LIMIT)
    return ((up_part + 1.0) * gate * jax.nn.sigmoid(ALPHA * gate)).astype(jnp.bfloat16)


def slot_numbers(id_blocks, experts, capacity):
    onehot = (id_blocks[:, :, None] == jnp.arange(experts, dtype=jnp.int32)[None, None, :]).astype(
        jnp.int32
    )
    before = jnp.cumsum(onehot, axis=1) - onehot
    position = jnp.sum(before * onehot, axis=2)
    return id_blocks * capacity + position


def project_down(hidden, down_weight):
    result = jnp.einsum(
        "sejf,efd->sejd",
        lax.all_gather(hidden, "tp", axis=3, tiled=True),
        down_weight,
        preferred_element_type=jnp.float32,
    )
    return result.astype(jnp.bfloat16)


def plain_path(tokens, expert_ids, route_weight, norm_gain, gate_weight, up_weight, down_weight):
    n_ep = lax.axis_size("ep")
    n_tp = lax.axis_size("tp")
    tok_rows, width = tokens.shape
    top = expert_ids.shape[1]
    local_experts = gate_weight.shape[0]
    experts = local_experts * n_ep
    capacity = 5 * tok_rows * top // (4 * experts)
    cols = width // n_tp
    normed = rms_norm(tokens, norm_gain)
    dest = slot_numbers(expert_ids.reshape(1, tok_rows * top), experts, capacity).reshape(-1)
    slot_range = jnp.arange(experts * capacity, dtype=jnp.int32)
    match = slot_range[:, None] == dest[None, :]
    pick = jnp.any(match.reshape(experts * capacity, tok_rows, top), axis=2).astype(jnp.bfloat16)
    own = lax.dynamic_slice_in_dim(normed, lax.axis_index("tp") * cols, cols, 1)
    buffer = jnp.dot(pick, own, preferred_element_type=jnp.float32).astype(jnp.bfloat16)
    buffer = buffer.reshape(n_ep, local_experts, capacity, cols)
    arrived = lax.all_to_all(buffer, "ep", split_axis=0, concat_axis=0, tiled=True)
    piece = lax.all_gather(arrived, "tp", axis=3, tiled=True)
    gate_part = jnp.einsum("sejd,edf->sejf", piece, gate_weight, preferred_element_type=jnp.float32)
    up_part = jnp.einsum("sejd,edf->sejf", piece, up_weight, preferred_element_type=jnp.float32)
    hidden = clamped_unit(gate_part, up_part)
    result = project_down(hidden, down_weight)
    back = lax.all_to_all(result, "ep", split_axis=0, concat_axis=0, tiled=True).reshape(
        experts * capacity, cols
    )
    chosen = jnp.transpose(match).astype(jnp.bfloat16)
    per_copy = jnp.dot(chosen, back, preferred_element_type=jnp.float32).reshape(
        tok_rows, top, cols
    )
    mixed = jnp.sum(per_copy * route_weight[:, :, None], axis=1)
    return mixed.astype(jnp.bfloat16)


VMEM_BYTES = 47 * 1024 * 1024
COLUMN_TILE = 256
PIECES = 2


def flip(value, bits):
    bit = 1
    while bit <= bits:
        if bits & bit:
            value = value + bit - 2 * bit * lax.rem(lax.div(value, jnp.int32(bit)), jnp.int32(2))
        bit *= 2
    return value


def fused_kernel(
    n_ep,
    n_tp,
    capacity,
    slots,
    tokens_hbm,
    ids_row_hbm,
    route_row_hbm,
    gain_hbm,
    gate_hbm,
    up_hbm,
    down_hbm,
    out_ref,
    tokens_ref,
    ids_row_ref,
    route_row_ref,
    gain_ref,
    gate_v,
    up_v,
    down_v,
    scales,
    normed,
    outbox,
    fullbox,
    zbox,
    zfull,
    xbuf,
    hbuf,
    obuf,
    back,
    acc,
    small_sem,
    weight_sem,
    z_send,
    z_recv,
    pair_send,
    pair_recv,
    g_send,
    g_recv,
    b_send,
    b_recv,
):
    pairs = n_ep // 2
    rows = 2 * capacity
    lead = slots - capacity
    second = rows - slots
    tok_rows, width = tokens_ref.shape
    cols = xbuf.shape[-1]
    hid = hbuf.shape[-1]
    outs = obuf.shape[-1]
    ep = lax.axis_index("ep")
    tp = lax.axis_index("tp")
    pair = lax.div(ep, jnp.int32(2))
    core = lax.rem(ep, jnp.int32(2))
    side = (flip(tp, 1), flip(tp, 2))
    far = flip(tp, 3)
    upper = lax.div(pair, jnp.int32(2))
    inner = lax.rem(pair + upper, jnp.int32(2))
    early, late = 2 + inner, 3 - inner
    chip_of = {0: pair, 1: flip(pair, 1), "early": 2 - upper, "late": 3 - 3 * upper}
    slot_of = {0: 0, 1: 1, "early": early, "late": late}

    small = (
        (tokens_hbm, tokens_ref),
        (ids_row_hbm, ids_row_ref),
        (route_row_hbm, route_row_ref),
        (gain_hbm, gain_ref),
    )
    small_loads = [
        pltpu.make_async_copy(a, b, small_sem.at[i]) for i, (a, b) in enumerate(small)
    ]
    for load in small_loads:
        load.start()
    loads = [
        pltpu.make_async_copy(hbm.at[0], vmem, weight_sem.at[i])
        for i, (hbm, vmem) in enumerate(((gate_hbm, gate_v), (up_hbm, up_v), (down_hbm, down_v)))
    ]

    barrier = pltpu.get_barrier_semaphore()
    for k in range(1, n_ep):
        pl.semaphore_signal(
            barrier, inc=1, device_id=(flip(ep, k), tp), device_id_type=pl.DeviceIdType.MESH
        )
    for other in side:
        pl.semaphore_signal(
            barrier, inc=1, device_id=(ep, other), device_id_type=pl.DeviceIdType.MESH
        )

    with jax.named_scope("small_wait"):
        for load in small_loads:
            load.wait()
    for load in loads:
        load.start()

    own_cols = pl.ds(pl.multiple_of(tp * cols, cols), cols)
    far_cols = pl.ds(pl.multiple_of(far * cols, cols), cols)

    def scale_rows(i, carry):
        at = pl.ds(pl.multiple_of(i * 32, 32), 32)
        values = tokens_ref[at, :].astype(jnp.float32)
        scale = lax.rsqrt(jnp.mean(values * values, axis=-1, keepdims=True) + EPS)
        scales[at, :] = jnp.broadcast_to(scale, (32, scales.shape[1]))
        for where in (own_cols, far_cols):
            values = tokens_ref[at, where].astype(jnp.float32)
            normed[at, where] = (values * scale * gain_ref[:, where]).astype(jnp.bfloat16)
        return carry

    with jax.named_scope("scale_rows"):
        lax.fori_loop(0, tok_rows // 32, scale_rows, 0)

    ids_row = ids_row_ref[...]
    expert_col = lax.broadcasted_iota(jnp.int32, (n_ep, tok_rows), 0)
    hits_row = ((ids_row[0:1, :] == expert_col) | (ids_row[1:2, :] == expert_col)).astype(
        jnp.float32
    ).astype(jnp.bfloat16)
    first = lax.broadcasted_iota(jnp.int32, (tok_rows, tok_rows), 0)
    second_at = lax.broadcasted_iota(jnp.int32, (tok_rows, tok_rows), 1)
    earlier = (first < second_at).astype(jnp.float32).astype(jnp.bfloat16)
    before_row = jnp.dot(hits_row, earlier, preferred_element_type=jnp.float32)
    slot_row = [
        jnp.sum(jnp.where(ids_row[k : k + 1, :] == expert_col, before_row, 0.0), axis=0, keepdims=True)
        for k in range(2)
    ]
    slot_at = (
        lax.broadcasted_iota(jnp.int32, (slots, tok_rows), 0) - lead * core
    ).astype(jnp.float32)

    def pick_of(expert):
        taken = ((ids_row[0:1, :] == expert) & (slot_row[0] == slot_at)) | (
            (ids_row[1:2, :] == expert) & (slot_row[1] == slot_at)
        )
        return taken.astype(jnp.float32).astype(jnp.bfloat16)

    def picked(pick, where):
        return jnp.dot(pick, normed[:, where], preferred_element_type=jnp.float32).astype(
            jnp.bfloat16
        )

    with jax.named_scope("barrier"):
        pl.semaphore_wait(barrier, n_ep - 1 + 2)

    box_cols = {0: tp, 1: far, 2: tp, 3: tp, 4: side[0], 5: side[1]}

    def box_flip(box):
        return box if box in (2, 3) else 1

    def z_copy(box, c):
        return pltpu.make_async_remote_copy(
            src_ref=outbox.at[box, c],
            dst_ref=zbox.at[box, core],
            send_sem=z_send.at[box, c],
            recv_sem=z_recv.at[box, core],
            device_id=(flip(pair, box_flip(box)) * 2 + c, tp),
            device_id_type=pl.DeviceIdType.MESH,
        )

    def z_wait(box, cs=(0, 1)):
        for c in cs:
            pltpu.make_async_remote_copy(
                src_ref=outbox.at[0, c],
                dst_ref=zbox.at[box, c],
                send_sem=z_send.at[0, c],
                recv_sem=z_recv.at[box, c],
                device_id=(flip(pair, 1) * 2 + c, tp),
                device_id_type=pl.DeviceIdType.MESH,
            ).wait_recv()

    def z_sends(boxes_in_order):
        for box in boxes_in_order:
            where = pl.ds(pl.multiple_of(box_cols[box] * cols, cols), cols)
            for c in range(2):
                pick = pick_of(flip(pair, box_flip(box)) * 2 + c)
                outbox[box, c] = picked(pick, where)
                z_copy(box, c).start()

    with jax.named_scope("z_sends"):
        pl.when(inner == 1)(lambda: z_sends((2, 3, 0, 1)))
        pl.when(inner == 0)(lambda: z_sends((0, 1, 2, 3)))

    def norm_rest(i, carry):
        at = pl.ds(pl.multiple_of(i * 32, 32), 32)
        for other in side:
            where = pl.ds(pl.multiple_of(other * cols, cols), cols)
            values = tokens_ref[at, where].astype(jnp.float32)
            normed[at, where] = (values * scales[at, 0:1] * gain_ref[:, where]).astype(
                jnp.bfloat16
            )
        return carry

    with jax.named_scope("norm_rest"):
        lax.fori_loop(0, tok_rows // 32, norm_rest, 0)

    partner = flip(ep, 1)

    def pair_copy(at):
        return pltpu.make_async_remote_copy(
            src_ref=fullbox,
            dst_ref=zfull.at[at],
            send_sem=pair_send,
            recv_sem=pair_recv,
            device_id=(partner, tp),
            device_id_type=pl.DeviceIdType.MESH,
        )

    with jax.named_scope("pair_pick"):
        theirs = pick_of(partner)
        for j in range(n_tp):
            fullbox[j] = picked(theirs, slice(j * cols, (j + 1) * cols))
        pair_copy(core).start()
        mine = pick_of(ep)
        for j in range(n_tp):
            zfull[core, j] = picked(mine, slice(j * cols, (j + 1) * cols))

    z_sends((4, 5))
    edge = slots - second

    def join(k, j, low, high):
        xbuf[k, j, 0:second, :] = low[0:second, :]
        xbuf[k, j, second:slots, :] = low[second:slots, :] + high[0:edge, :]
        xbuf[k, j, slots:rows, :] = high[edge:slots, :]

    boxes = (xbuf, hbuf)
    half_cols = cols // 2
    spans = {0: (0, slots), 1: (slots, rows), None: (0, rows)}
    both = (0, 1)
    whole = (None,)
    far_parts = whole

    def g_copy(b, k, j, half, r, to, at):
        start, stop = spans[r]
        where = boxes[b].at[k, j, pl.ds(start, stop - start), pl.ds(half * half_cols, half_cols)]
        r = r or 0
        return pltpu.make_async_remote_copy(
            src_ref=where,
            dst_ref=where,
            send_sem=g_send.at[b, k, r, at],
            recv_sem=g_recv.at[b, k, r, at],
            device_id=(ep, to),
            device_id_type=pl.DeviceIdType.MESH,
        )

    def block_copy(b, k, d, half, r):
        return g_copy(b, k, tp, half, r, side[d], 2 * d + half)

    def block_arrival(b, k, d, half, r):
        return g_copy(b, k, side[d], half, r, side[d], 2 * d + half)

    def relay_copy(b, k, d, r):
        return g_copy(b, k, side[d], d, r, side[1 - d], 4 + d)

    def relay_arrival(b, k, d, r):
        return g_copy(b, k, far, d, r, side[1 - d], 4 + d)

    def spread_half(b, k, half, rs=whole):
        for r in rs:
            for d in range(2):
                block_copy(b, k, d, half, r).start()

    def spread(b, k, rs=whole):
        for r in rs:
            for step in range(2):
                for d in range(2):
                    block_copy(b, k, d, d if step == 0 else 1 - d, r).start()

    def relay(b, k, rs=whole, ds=both):
        for r in rs:
            for d in ds:
                with jax.named_scope(f"w_relay_{b}_{r}"):
                    block_arrival(b, k, d, d, r).wait_recv()
                relay_copy(b, k, d, r).start()

    def near(b, k, rs=whole):
        for r in rs:
            with jax.named_scope(f"w_near_{b}_{r}"):
                for d in range(2):
                    block_arrival(b, k, d, 1 - d, r).wait_recv()

    def distant(b, k, rs=whole):
        for r in rs:
            with jax.named_scope(f"w_far_{b}_{r}"):
                for d in range(2):
                    relay_arrival(b, k, d, r).wait_recv()

    def enter(k, rs=whole, wait=True):
        if wait:
            with jax.named_scope("w_z"):
                z_wait(k)
        join(k, tp, zbox[k, 0], zbox[k, 1])
        spread(0, k, rs)

    def enter_next():
        for box in (0, 1, 4, 5):
            with jax.named_scope("w_z1"):
                z_wait(box)
            join(1, box_cols[box], zbox[box, 0], zbox[box, 1])

    def dot_blocks(box, k, r, weight, where, blocks):
        depth = box.shape[-1]
        start, stop = spans[r]
        total = None
        for j in blocks:
            at = j * depth if isinstance(j, int) else pl.multiple_of(j * depth, depth)
            part = jnp.dot(
                box[k, j, start:stop, :], weight[pl.ds(at, depth), where],
                preferred_element_type=jnp.float32,
            )
            total = part if total is None else total + part
        return total

    every = tuple(range(n_tp))
    close = (tp,) + side

    def column(i):
        return pl.ds(pl.multiple_of(i * COLUMN_TILE, COLUMN_TILE), COLUMN_TILE)

    def units(k, part, r=None, parts=2, stage=None):
        start, stop = spans[r]
        blocks = {None: every, 0: close, 1: (far,)}[stage]

        def tile(i, carry):
            where = column(i)
            gate_pre = dot_blocks(xbuf, k, r, gate_v, where, blocks)
            up_pre = dot_blocks(xbuf, k, r, up_v, where, blocks)
            if stage == 0:
                acc[0, start:stop, where] = gate_pre
                acc[1, start:stop, where] = up_pre
                return carry
            if stage == 1:
                gate_pre = gate_pre + acc[0, start:stop, where]
                up_pre = up_pre + acc[1, start:stop, where]
            hbuf[k, tp, start:stop, where] = clamped_unit(gate_pre, up_pre)
            return carry

        tiles = hid // COLUMN_TILE // parts
        with jax.named_scope(f"units_{stage}_{r}"):
            lax.fori_loop(part * tiles, (part + 1) * tiles, tile, 0)

    def produce(k, r=None, stage=None):
        for half in range(2):
            units(k, half, r, 2, stage)
            spread_half(1, k, half, (r,))

    piece = outs // PIECES

    def piece_of(ref, at):
        return ref.at[:, pl.ds(at * piece, piece)]

    def back_copy(name, c, at):
        k = slot_of[name]
        return pltpu.make_async_remote_copy(
            src_ref=obuf.at[k, pl.ds(second * c, slots), pl.ds(at * piece, piece)],
            dst_ref=back.at[ep, :, pl.ds(at * piece, piece)],
            send_sem=b_send.at[k, c, at],
            recv_sem=b_recv.at[ep, at],
            device_id=(chip_of[name] * 2 + c, tp),
            device_id_type=pl.DeviceIdType.MESH,
        )

    def partner_copy(at):
        return pltpu.make_async_remote_copy(
            src_ref=obuf.at[
                0, pl.ds(pl.multiple_of(second * (1 - core), 8), slots), pl.ds(at * piece, piece)
            ],
            dst_ref=back.at[ep, :, pl.ds(at * piece, piece)],
            send_sem=b_send.at[0, 0, at],
            recv_sem=b_recv.at[ep, at],
            device_id=(partner, tp),
            device_id_type=pl.DeviceIdType.MESH,
        )

    def back_arrival(flips, at):
        other = flip(ep, flips)
        return pltpu.make_async_remote_copy(
            src_ref=obuf.at[0, pl.ds(0, slots), pl.ds(at * piece, piece)],
            dst_ref=back.at[other, :, pl.ds(at * piece, piece)],
            send_sem=b_send.at[0, 0, at],
            recv_sem=b_recv.at[other, at],
            device_id=(other, tp),
            device_id_type=pl.DeviceIdType.MESH,
        )

    def results(name, r=None, stage=None):
        k = slot_of[name]
        start, stop = spans[r]
        blocks = {None: every, 0: close, 1: (far,)}[stage]

        def tile(i, carry):
            where = column(i)
            total = dot_blocks(hbuf, k, r, down_v, where, blocks)
            if stage == 0:
                acc[2, start:stop, where] = total
                return carry
            if stage == 1:
                total = total + acc[2, start:stop, where]
            obuf[k, start:stop, where] = total.astype(jnp.bfloat16)
            return carry

        tiles = outs // COLUMN_TILE // PIECES
        for at in range(PIECES):
            with jax.named_scope(f"results_{name}_{stage}_{r}"):
                lax.fori_loop(at * tiles, (at + 1) * tiles, tile, 0)
            if stage == 0:
                continue
            if name == 0:
                partner_copy(at).start()
            else:
                for c in both if r is None else (r,):
                    back_copy(name, c, at).start()
        if name == 0 and stage != 0:
            back[ep] = obuf[0, pl.ds(pl.multiple_of(second * core, 8), slots), :]

    def begin(name, r=None):
        near(1, slot_of[name], (r,))
        results(name, r, 0)

    def finish(name, r=None):
        distant(1, slot_of[name], (r,))
        results(name, r, 1)

    with jax.named_scope("w_pair"):
        pair_copy(1 - core).wait_recv()
    for j in range(n_tp):
        join(0, j, zfull[0, j], zfull[1, j])
    with jax.named_scope("w_gateup"):
        loads[0].wait()
        loads[1].wait()
    units(0, 0)
    spread_half(1, 0, 0)
    units(0, 1)

    def outer_order():
        enter(2)
        relay(0, 2)
        near(0, 2)
        spread_half(1, 0, 1)
        units(2, 0, None, 1, 0)
        distant(0, 2)
        produce(2, None, 1)
        relay(1, 2)
        enter(3)
        loads[2].wait()
        begin("early")
        finish("early")
        relay(0, 3)
        relay(1, 0)
        near(0, 3)
        units(3, 0, None, 1, 0)
        distant(0, 3)
        produce(3, None, 1)
        enter_next()
        produce(1)
        relay(1, 3)
        begin("late")
        finish("late")
        relay(1, 1)
        begin(1)
        finish(1)
        begin(0)
        finish(0)

    def inner_order():
        enter(3)
        relay(0, 3)
        near(0, 3)
        spread_half(1, 0, 1)
        units(3, 0, None, 1, 0)
        distant(0, 3)
        produce(3, None, 1)
        relay(1, 3)
        enter(2)
        loads[2].wait()
        begin("early")
        finish("early")
        relay(0, 2)
        relay(1, 0)
        near(0, 2)
        units(2, 0, None, 1, 0)
        distant(0, 2)
        produce(2, None, 1)
        enter_next()
        produce(1)
        relay(1, 2)
        begin("late")
        finish("late")
        relay(1, 1)
        begin(1)
        finish(1)
        begin(0)
        finish(0)

    pl.when(inner == 0)(outer_order)
    pl.when(inner == 1)(inner_order)

    place = lax.broadcasted_iota(jnp.int32, (n_ep * slots, tok_rows), 0).astype(jnp.float32)
    share = None
    for k in range(2):
        spot = (
            ids_row[k : k + 1, :].astype(jnp.float32) * slots
            + slot_row[k]
            + (lead * core).astype(jnp.float32)
        )
        part = jnp.where(place == spot, route_row_ref[k : k + 1, :], 0.0)
        share = part if share is None else share + part
    share = jnp.transpose(share)
    share_high = share.astype(jnp.bfloat16)
    share_low = (share - share_high.astype(jnp.float32)).astype(jnp.bfloat16)

    with jax.named_scope("w_sends"):
        for box in range(6):
            for c in range(2):
                z_copy(box, c).wait_send()
        pair_copy(core).wait_send()
        for k in range(pairs):
            for b in range(2):
                if b == 0 and k < 2:
                    continue
                for d in range(2):
                    for r in far_parts if k > 1 else whole:
                        for half in range(2):
                            block_copy(b, k, d, half, r).wait_send()
                        relay_copy(b, k, d, r).wait_send()
        for at in range(PIECES):
            partner_copy(at).wait_send()
            for name in (1, "early", "late"):
                for c in range(2):
                    back_copy(name, c, at).wait_send()

    with jax.named_scope("w_back"):
        for at in range(PIECES):
            for flips in range(1, n_ep):
                back_arrival(flips, at).wait_recv()

    def mix(i, carry):
        where = pl.ds(pl.multiple_of(i * COLUMN_TILE, COLUMN_TILE), COLUMN_TILE)
        table = back[:, :, where].reshape(n_ep * slots, COLUMN_TILE)
        total = jnp.dot(share_high, table, preferred_element_type=jnp.float32)
        total = total + jnp.dot(share_low, table, preferred_element_type=jnp.float32)
        out_ref[:, where] = total.astype(jnp.bfloat16)
        return carry

    with jax.named_scope("mix"):
        lax.fori_loop(0, outs // COLUMN_TILE, mix, 0)


def fused_path(
    n_ep, n_tp, tokens, expert_ids, route_weight, norm_gain, gate_weight, up_weight, down_weight
):
    tok_rows, width = tokens.shape
    capacity, slots = slots_of(n_ep, tokens.shape, expert_ids.shape)
    rows = 2 * capacity
    hid = gate_weight.shape[2]
    outs = down_weight.shape[2]
    cols = width // n_tp
    pairs = n_ep // 2
    vmem = pl.BlockSpec(memory_space=pltpu.VMEM)
    hbm = pl.BlockSpec(memory_space=pltpu.HBM)
    dma = pltpu.SemaphoreType.DMA
    arrays = (
        tokens,
        jnp.transpose(expert_ids),
        jnp.transpose(route_weight),
        norm_gain.reshape(1, width),
        gate_weight,
        up_weight,
        down_weight,
    )
    return pl.pallas_call(
        functools.partial(fused_kernel, n_ep, n_tp, capacity, slots),
        out_shape=jax.ShapeDtypeStruct((tok_rows, outs), jnp.bfloat16),
        in_specs=[hbm] * 7,
        out_specs=vmem,
        scratch_shapes=[
            pltpu.VMEM(tokens.shape, tokens.dtype),
            pltpu.VMEM(expert_ids.shape[::-1], expert_ids.dtype),
            pltpu.VMEM(route_weight.shape[::-1], route_weight.dtype),
            pltpu.VMEM((1, width), norm_gain.dtype),
            pltpu.VMEM(gate_weight.shape[1:], jnp.bfloat16),
            pltpu.VMEM(up_weight.shape[1:], jnp.bfloat16),
            pltpu.VMEM(down_weight.shape[1:], jnp.bfloat16),
            pltpu.VMEM((tok_rows, 128), jnp.float32),
            pltpu.VMEM((tok_rows, width), jnp.bfloat16),
            pltpu.VMEM((pairs + 2, 2, slots, cols), jnp.bfloat16),
            pltpu.VMEM((n_tp, slots, cols), jnp.bfloat16),
            pltpu.VMEM((pairs + 2, 2, slots, cols), jnp.bfloat16),
            pltpu.VMEM((2, n_tp, slots, cols), jnp.bfloat16),
            pltpu.VMEM((pairs, n_tp, rows, cols), jnp.bfloat16),
            pltpu.VMEM((pairs, n_tp, rows, hid), jnp.bfloat16),
            pltpu.VMEM((pairs, rows, outs), jnp.bfloat16),
            pltpu.VMEM((n_ep, slots, outs), jnp.bfloat16),
            pltpu.VMEM((3, rows, hid), jnp.float32),
            dma((4,)),
            dma((3,)),
            dma((pairs + 2, 2)),
            dma((pairs + 2, 2)),
            dma,
            dma,
            dma((2, pairs, 2, 6)),
            dma((2, pairs, 2, 6)),
            dma((pairs, 2, PIECES)),
            dma((n_ep, PIECES)),
        ],
        compiler_params=pltpu.CompilerParams(
            collective_id=0, has_side_effects=True, vmem_limit_bytes=VMEM_BYTES
        ),
    )(*(pltpu.with_memory_space_constraint(array, pltpu.HBM) for array in arrays))


def slots_of(n_ep, token_shape, id_shape):
    capacity = 5 * token_shape[0] * id_shape[1] // (4 * n_ep)
    return capacity, -(-capacity // 8) * 8


def on_device(tokens, expert_ids, route_weight, norm_gain, gate_weight, up_weight, down_weight):
    n_ep = lax.axis_size("ep")
    n_tp = lax.axis_size("tp")
    args = (tokens, expert_ids, route_weight, norm_gain, gate_weight, up_weight, down_weight)
    fits = n_tp == 4 and n_ep == 8 and gate_weight.shape[0] == 1 and expert_ids.shape[1] == 2
    capacity, slots = slots_of(n_ep, tokens.shape, expert_ids.shape)
    if fits and capacity % 4 == 0 and slots > capacity:
        return fused_path(n_ep, n_tp, *args)
    return plain_path(*args)


def solution(mesh):
    placed = (
        P("ep", None),
        P("ep", None),
        P("ep", None),
        P(),
        P("ep", None, "tp"),
        P("ep", None, "tp"),
        P("ep", None, "tp"),
    )
    return jax.shard_map(
        on_device, mesh=mesh, in_specs=placed, out_specs=P("ep", "tp"), check_vma=False
    )
```

time: 94.3 us -> 82.1 us (0.87); the launches traced: 93 us -> 82 us
  Pallas kernels: 92.3 us -> 81.2 us
    pallas_call x1, Pallas kernels: 92.3 us -> 81.2 us  [fused_path(): pl.pallas_call(functools.partial(fused_kernel, n_ep, n_tp, capacity, slot...]
where the time goes in v1:
time: 82.1 us; the launch traced here: 82 us
  Pallas kernels  81.2 us (99%)
    pallas_call x1, Pallas kernels, fused_path(): pl.pallas_call(functools.partial(fused_kernel, n_ep, n_tp, capacity, slot...  81.2 us

profile of v1, /device:TPU:1, one launch (start us, length us, event | category | flops | bytes accessed | tf_op | source)
XLA Modules:
  0.0 82.0 jit_solution(11539678275083355654)
XLA Ops:
  0.0 81.2 %shard_map.73 = bf16[192,1024]{1,0:T(8,128)(2,1)S(1)} custom-call(bf16[192,4096]{1,0:T(8,128)(2,1)} %tokens_hbm.1, s32[2,192]{1,0:T(2,128)} %bitcast.4, f32[2,192]{1,0:T(2,128)} %bitcast.5, f32[1,4096]{1,0:T(1,128)} %bitcast.3, bf16[1,4096,1024]{2,1,0:T(8,128)(2,1)} %gate_hbm.1, bf16[1,4096,1024]{2,1,0:T(8,128)(2,1)} %up_hbm.1, bf16[1,4096,1024]{2,1,0:T(8,128)(2,1)} %down_hbm.1), custom_call_target="tpu_custom_call" | custom-call | tf_op jit(solution)/shard_map/pallas_call | solution.py:660
  81.2 0.7 copy.9

commit v2 on v1

--- a/solution.py
+++ b/solution.py
@@ -122,6 +122,7 @@
     obuf,
     back,
     acc,
+    mixed,
     small_sem,
     weight_sem,
     z_send,
@@ -147,11 +148,8 @@
     core = lax.rem(ep, jnp.int32(2))
     side = (flip(tp, 1), flip(tp, 2))
     far = flip(tp, 3)
-    upper = lax.div(pair, jnp.int32(2))
-    inner = lax.rem(pair + upper, jnp.int32(2))
-    early, late = 2 + inner, 3 - inner
-    chip_of = {0: pair, 1: flip(pair, 1), "early": 2 - upper, "late": 3 - 3 * upper}
-    slot_of = {0: 0, 1: 1, "early": early, "late": late}
+    inner = lax.rem(pair + lax.div(pair, jnp.int32(2)), jnp.int32(2))
+    chip_of = [flip(pair, k) for k in range(pairs)]
 
     small = (
         (tokens_hbm, tokens_ref),
@@ -232,31 +230,33 @@
     with jax.named_scope("barrier"):
         pl.semaphore_wait(barrier, n_ep - 1 + 2)
 
-    box_cols = {0: tp, 1: far, 2: tp, 3: tp, 4: side[0], 5: side[1]}
+    box_cols = (tp, tp, tp, far) + side + (far,)
 
     def box_flip(box):
-        return box if box in (2, 3) else 1
+        return {0: 2, 1: 3, 6: 3}.get(box, 1)
 
     def z_copy(box, c):
         return pltpu.make_async_remote_copy(
             src_ref=outbox.at[box, c],
             dst_ref=zbox.at[box, core],
-            send_sem=z_send.at[box, c],
-            recv_sem=z_recv.at[box, core],
+            send_sem=z_send,
+            recv_sem=z_recv.at[(0, 1, 2, 2, 3, 3, 4)[box]],
             device_id=(flip(pair, box_flip(box)) * 2 + c, tp),
             device_id_type=pl.DeviceIdType.MESH,
         )
 
-    def z_wait(box, cs=(0, 1)):
-        for c in cs:
-            pltpu.make_async_remote_copy(
-                src_ref=outbox.at[0, c],
-                dst_ref=zbox.at[box, c],
-                send_sem=z_send.at[0, c],
-                recv_sem=z_recv.at[box, c],
-                device_id=(flip(pair, 1) * 2 + c, tp),
-                device_id_type=pl.DeviceIdType.MESH,
-            ).wait_recv()
+    def bytes_of(ref, send, recv):
+        return pltpu.make_async_remote_copy(
+            src_ref=ref,
+            dst_ref=ref,
+            send_sem=send,
+            recv_sem=recv,
+            device_id=(ep, side[0]),
+            device_id_type=pl.DeviceIdType.MESH,
+        )
+
+    def z_wait(at, ref):
+        bytes_of(ref, z_send, z_recv.at[at]).wait_recv()
 
     def z_sends(boxes_in_order):
         for box in boxes_in_order:
@@ -267,8 +267,8 @@
                 z_copy(box, c).start()
 
     with jax.named_scope("z_sends"):
-        pl.when(inner == 1)(lambda: z_sends((2, 3, 0, 1)))
-        pl.when(inner == 0)(lambda: z_sends((0, 1, 2, 3)))
+        pl.when(inner == 1)(lambda: z_sends((0, 1, 2)))
+        pl.when(inner == 0)(lambda: z_sends((2, 0, 3, 1)))
 
     def norm_rest(i, carry):
         at = pl.ds(pl.multiple_of(i * 32, 32), 32)
@@ -304,7 +304,6 @@
         for j in range(n_tp):
             zfull[core, j] = picked(mine, slice(j * cols, (j + 1) * cols))
 
-    z_sends((4, 5))
     edge = slots - second
 
     def join(k, j, low, high):
@@ -316,75 +315,86 @@
     half_cols = cols // 2
     spans = {0: (0, slots), 1: (slots, rows), None: (0, rows)}
     both = (0, 1)
-    whole = (None,)
-    far_parts = whole
-
-    def g_copy(b, k, j, half, r, to, at):
+
+    def group(b, k, r):
+        return k - 2 if b == 0 else 2 + 2 * k + (r or 0)
+
+    def g_copy(b, k, j, half, r, to, kind):
         start, stop = spans[r]
         where = boxes[b].at[k, j, pl.ds(start, stop - start), pl.ds(half * half_cols, half_cols)]
-        r = r or 0
         return pltpu.make_async_remote_copy(
             src_ref=where,
             dst_ref=where,
-            send_sem=g_send.at[b, k, r, at],
-            recv_sem=g_recv.at[b, k, r, at],
+            send_sem=g_send.at[b, k],
+            recv_sem=g_recv.at[group(b, k, r), kind],
             device_id=(ep, to),
             device_id_type=pl.DeviceIdType.MESH,
         )
 
     def block_copy(b, k, d, half, r):
-        return g_copy(b, k, tp, half, r, side[d], 2 * d + half)
-
-    def block_arrival(b, k, d, half, r):
-        return g_copy(b, k, side[d], half, r, side[d], 2 * d + half)
-
-    def relay_copy(b, k, d, r):
-        return g_copy(b, k, side[d], d, r, side[1 - d], 4 + d)
-
-    def relay_arrival(b, k, d, r):
-        return g_copy(b, k, far, d, r, side[1 - d], 4 + d)
-
-    def spread_half(b, k, half, rs=whole):
-        for r in rs:
-            for d in range(2):
-                block_copy(b, k, d, half, r).start()
-
-    def spread(b, k, rs=whole):
-        for r in rs:
-            for step in range(2):
-                for d in range(2):
-                    block_copy(b, k, d, d if step == 0 else 1 - d, r).start()
-
-    def relay(b, k, rs=whole, ds=both):
-        for r in rs:
-            for d in ds:
-                with jax.named_scope(f"w_relay_{b}_{r}"):
-                    block_arrival(b, k, d, d, r).wait_recv()
-                relay_copy(b, k, d, r).start()
-
-    def near(b, k, rs=whole):
-        for r in rs:
-            with jax.named_scope(f"w_near_{b}_{r}"):
-                for d in range(2):
-                    block_arrival(b, k, d, 1 - d, r).wait_recv()
-
-    def distant(b, k, rs=whole):
-        for r in rs:
-            with jax.named_scope(f"w_far_{b}_{r}"):
-                for d in range(2):
-                    relay_arrival(b, k, d, r).wait_recv()
-
-    def enter(k, rs=whole, wait=True):
-        if wait:
-            with jax.named_scope("w_z"):
-                z_wait(k)
-        join(k, tp, zbox[k, 0], zbox[k, 1])
-        spread(0, k, rs)
-
-    def enter_next():
-        for box in (0, 1, 4, 5):
-            with jax.named_scope("w_z1"):
-                z_wait(box)
+        return g_copy(b, k, tp, half, r, side[d], d if half == d and (b, k) != (0, 3) else 2)
+
+    def take(b, k, r=None):
+        for d in range(2):
+            with jax.named_scope(f"w_relay_{b}_{r}"):
+                g_copy(b, k, side[d], d, r, side[d], d).wait_recv()
+
+    def hand(b, k, r=None):
+        for d in range(2):
+            g_copy(b, k, side[d], d, r, side[1 - d], 3).start()
+
+    def relay(b, k, r=None):
+        for d in range(2):
+            with jax.named_scope(f"w_relay_{b}_{r}"):
+                g_copy(b, k, side[d], d, r, side[d], d).wait_recv()
+            g_copy(b, k, side[d], d, r, side[1 - d], 3).start()
+
+    def arrive(b, k, r, kind):
+        start, stop = spans[r]
+        where = boxes[b].at[k, far, pl.ds(start, stop - start), :]
+        bytes_of(where, g_send.at[b, k], g_recv.at[group(b, k, r), kind]).wait_recv()
+
+    def send_half(b, k, half, r=None):
+        for d in range(2):
+            block_copy(b, k, d, half, r).start()
+
+    def send_first(b, k, r=None):
+        for d in range(2):
+            block_copy(b, k, d, d, r).start()
+
+    def send_rest(b, k, r=None):
+        for d in range(2):
+            block_copy(b, k, d, 1 - d, r).start()
+
+    def spread(b, k, r=None):
+        send_first(b, k, r)
+        send_rest(b, k, r)
+
+    def near(b, k, r=None):
+        with jax.named_scope(f"w_near_{b}_{r}"):
+            if (b, k) == (0, 3):
+                bytes_of(xbuf.at[k, pl.ds(0, 2)], g_send.at[b, k], g_recv.at[1, 2]).wait_recv()
+            else:
+                arrive(b, k, r, 2)
+
+    def distant(b, k, r=None):
+        with jax.named_scope(f"w_far_{b}_{r}"):
+            arrive(b, k, r, 3)
+
+    def enter(k):
+        with jax.named_scope("w_z"):
+            z_wait(k - 2, zbox.at[k - 2])
+        join(k, tp, zbox[k - 2, 0], zbox[k - 2, 1])
+
+    def enter_far():
+        with jax.named_scope("w_zfar"):
+            z_wait(4, zbox.at[6])
+        join(3, far, zbox[6, 0], zbox[6, 1])
+
+    def enter_next(part):
+        with jax.named_scope(f"w_z1_{part}"):
+            z_wait(2 + part, zbox.at[pl.ds(2 + 2 * part, 2)])
+        for box in range(2 + 2 * part, 4 + 2 * part):
             join(1, box_cols[box], zbox[box, 0], zbox[box, 1])
 
     def dot_blocks(box, k, r, weight, where, blocks):
@@ -406,85 +416,71 @@
     def column(i):
         return pl.ds(pl.multiple_of(i * COLUMN_TILE, COLUMN_TILE), COLUMN_TILE)
 
-    def units(k, part, r=None, parts=2, stage=None):
-        start, stop = spans[r]
-        blocks = {None: every, 0: close, 1: (far,)}[stage]
+    stages = {
+        None: (every, None, None),
+        "near": (close, None, 0),
+        "far": ((far,), 0, None),
+        "own": ((tp, far), None, 2),
+        "side": (side, 2, None),
+        "own_last": ((tp, far), None, 0),
+        "side_last": (side, 0, None),
+    }
+
+    def units(k, stage=None, halves=both):
+        blocks, start, keep = stages[stage]
 
         def tile(i, carry):
             where = column(i)
-            gate_pre = dot_blocks(xbuf, k, r, gate_v, where, blocks)
-            up_pre = dot_blocks(xbuf, k, r, up_v, where, blocks)
-            if stage == 0:
-                acc[0, start:stop, where] = gate_pre
-                acc[1, start:stop, where] = up_pre
-                return carry
-            if stage == 1:
-                gate_pre = gate_pre + acc[0, start:stop, where]
-                up_pre = up_pre + acc[1, start:stop, where]
-            hbuf[k, tp, start:stop, where] = clamped_unit(gate_pre, up_pre)
+            gate_pre = dot_blocks(xbuf, k, None, gate_v, where, blocks)
+            up_pre = dot_blocks(xbuf, k, None, up_v, where, blocks)
+            if start is not None:
+                gate_pre = gate_pre + acc[start, :, where]
+                up_pre = up_pre + acc[start + 1, :, where]
+            if keep is not None:
+                acc[keep, :, where] = gate_pre
+                acc[keep + 1, :, where] = up_pre
+            else:
+                hbuf[k, tp, :, where] = clamped_unit(gate_pre, up_pre)
             return carry
 
-        tiles = hid // COLUMN_TILE // parts
-        with jax.named_scope(f"units_{stage}_{r}"):
-            lax.fori_loop(part * tiles, (part + 1) * tiles, tile, 0)
-
-    def produce(k, r=None, stage=None):
-        for half in range(2):
-            units(k, half, r, 2, stage)
-            spread_half(1, k, half, (r,))
+        tiles = hid // COLUMN_TILE // 2
+        with jax.named_scope(f"units_{stage}"):
+            lax.fori_loop(halves[0] * tiles, (halves[-1] + 1) * tiles, tile, 0)
+
+    def produce(k, stage, r=None):
+        for half in both:
+            units(k, stage, (half,))
+            block_copy(1, k, half, half, r).start()
+        send_rest(1, k, r)
 
     piece = outs // PIECES
 
     def piece_of(ref, at):
         return ref.at[:, pl.ds(at * piece, piece)]
 
-    def back_copy(name, c, at):
-        k = slot_of[name]
+    def back_send(k, start, to, at, group_at):
         return pltpu.make_async_remote_copy(
-            src_ref=obuf.at[k, pl.ds(second * c, slots), pl.ds(at * piece, piece)],
+            src_ref=obuf.at[k, pl.ds(start, slots), pl.ds(at * piece, piece)],
             dst_ref=back.at[ep, :, pl.ds(at * piece, piece)],
-            send_sem=b_send.at[k, c, at],
-            recv_sem=b_recv.at[ep, at],
-            device_id=(chip_of[name] * 2 + c, tp),
+            send_sem=b_send,
+            recv_sem=b_recv.at[group_at],
+            device_id=(to, tp),
             device_id_type=pl.DeviceIdType.MESH,
         )
 
-    def partner_copy(at):
-        return pltpu.make_async_remote_copy(
-            src_ref=obuf.at[
-                0, pl.ds(pl.multiple_of(second * (1 - core), 8), slots), pl.ds(at * piece, piece)
-            ],
-            dst_ref=back.at[ep, :, pl.ds(at * piece, piece)],
-            send_sem=b_send.at[0, 0, at],
-            recv_sem=b_recv.at[ep, at],
-            device_id=(partner, tp),
-            device_id_type=pl.DeviceIdType.MESH,
-        )
-
-    def back_arrival(flips, at):
-        other = flip(ep, flips)
-        return pltpu.make_async_remote_copy(
-            src_ref=obuf.at[0, pl.ds(0, slots), pl.ds(at * piece, piece)],
-            dst_ref=back.at[other, :, pl.ds(at * piece, piece)],
-            send_sem=b_send.at[0, 0, at],
-            recv_sem=b_recv.at[other, at],
-            device_id=(other, tp),
-            device_id_type=pl.DeviceIdType.MESH,
-        )
-
-    def results(name, r=None, stage=None):
-        k = slot_of[name]
+    def results(name, stage, r=None):
+        k = name
         start, stop = spans[r]
-        blocks = {None: every, 0: close, 1: (far,)}[stage]
+        blocks, _, keep = stages[stage]
+        at_acc = 5 if name == 0 else 4
 
         def tile(i, carry):
             where = column(i)
             total = dot_blocks(hbuf, k, r, down_v, where, blocks)
-            if stage == 0:
-                acc[2, start:stop, where] = total
+            if keep is not None:
+                acc[at_acc, start:stop, where] = total
                 return carry
-            if stage == 1:
-                total = total + acc[2, start:stop, where]
+            total = total + acc[at_acc, start:stop, where]
             obuf[k, start:stop, where] = total.astype(jnp.bfloat16)
             return carry
 
@@ -492,23 +488,71 @@
         for at in range(PIECES):
             with jax.named_scope(f"results_{name}_{stage}_{r}"):
                 lax.fori_loop(at * tiles, (at + 1) * tiles, tile, 0)
-            if stage == 0:
+            if keep is not None:
                 continue
             if name == 0:
-                partner_copy(at).start()
+                back_send(0, pl.multiple_of(second * (1 - core), 8), partner, at, 0).start()
             else:
                 for c in both if r is None else (r,):
-                    back_copy(name, c, at).start()
-        if name == 0 and stage != 0:
+                    back_send(k, second * c, chip_of[name] * 2 + c, at, int(name == 1)).start()
+        if name == 0 and keep is None:
             back[ep] = obuf[0, pl.ds(pl.multiple_of(second * core, 8), slots), :]
 
     def begin(name, r=None):
-        near(1, slot_of[name], (r,))
-        results(name, r, 0)
+        near(1, name, r)
+        results(name, "near", r)
 
     def finish(name, r=None):
-        distant(1, slot_of[name], (r,))
-        results(name, r, 1)
+        distant(1, name, r)
+        results(name, "far", r)
+
+    mixed_chips = ((pair, chip_of[2], chip_of[3]), (chip_of[1],))
+
+    def share_of(part):
+        place = lax.broadcasted_iota(jnp.int32, (slots, tok_rows), 0)
+        shares = []
+        for chip in mixed_chips[part]:
+            for c in both:
+                share = None
+                for k in range(2):
+                    hit = (ids_row[k : k + 1, :] == chip * 2 + c) & (slot_row[k] == slot_at)
+                    one = jnp.where(hit, route_row_ref[k : k + 1, :], 0.0)
+                    share = one if share is None else share + one
+                shares.append(share)
+        share = jnp.transpose(jnp.concatenate(shares, axis=0))
+        high = share.astype(jnp.bfloat16)
+        low = (share - high.astype(jnp.float32)).astype(jnp.bfloat16)
+        return jnp.concatenate([high, low], axis=1)
+
+    def mix(part):
+        share = share_of(part)
+        with jax.named_scope(f"w_back_{part}"):
+            got = back.at[pl.ds(0, 2 if part else 5)]
+            bytes_of(got, b_send, b_recv.at[part]).wait_recv()
+
+        def tile(i, carry):
+            where = column(i)
+            blocks = [back[chip * 2 + c, :, where] for chip in mixed_chips[part] for c in both]
+            table = jnp.concatenate(blocks + blocks, axis=0)
+            total = jnp.dot(share, table, preferred_element_type=jnp.float32)
+            if part == 0:
+                mixed[:, where] = total
+            else:
+                out_ref[:, where] = (mixed[:, where] + total).astype(jnp.bfloat16)
+            return carry
+
+        with jax.named_scope(f"mix_{part}"):
+            lax.fori_loop(0, outs // COLUMN_TILE, tile, 0, unroll=True)
+
+    def sends_done():
+        with jax.named_scope("w_sends"):
+            bytes_of(outbox, z_send, z_recv.at[0]).wait_send()
+            pair_copy(core).wait_send()
+            for b in range(2):
+                for k in range(2 - 2 * b, pairs):
+                    if (b, k) != (1, 1):
+                        sent = boxes[b].at[k, pl.ds(0, 2 if (b, k) == (0, 3) else 3)]
+                        bytes_of(sent, g_send.at[b, k], g_recv.at[0, 0]).wait_send()
 
     with jax.named_scope("w_pair"):
         pair_copy(1 - core).wait_recv()
@@ -517,122 +561,115 @@
     with jax.named_scope("w_gateup"):
         loads[0].wait()
         loads[1].wait()
-    units(0, 0)
-    spread_half(1, 0, 0)
-    units(0, 1)
+    pl.when(inner == 1)(lambda: z_sends((3, 6)))
+    units(0, None, (0,))
+    send_half(1, 0, 0)
+    units(0, None, (1,))
 
     def outer_order():
+        z_sends((6, 4, 5))
         enter(2)
+        spread(0, 2)
         relay(0, 2)
         near(0, 2)
-        spread_half(1, 0, 1)
-        units(2, 0, None, 1, 0)
+        send_half(1, 0, 1)
+        units(2, "near")
         distant(0, 2)
-        produce(2, None, 1)
+        produce(2, "far")
+        enter_next(0)
+        units(1, "own")
+        loads[2].wait()
+        take(1, 0)
+        begin(0)
         relay(1, 2)
         enter(3)
+        spread(0, 3)
+        begin(2)
+        finish(2)
+        enter_far()
+        units(3, "own_last")
+        hand(1, 0)
+        near(0, 3)
+        produce(3, "side_last", 0)
+        send_first(1, 3, 1)
+        relay(1, 3, 0)
+        send_rest(1, 3, 1)
+        enter_next(1)
+        units(1, "side")
+        relay(1, 3, 1)
+        spread(1, 1, 0)
+        send_first(1, 1, 1)
+        begin(3, 0)
+        finish(3, 0)
+        begin(3, 1)
+        finish(3, 1)
+        relay(1, 1, 0)
+        send_rest(1, 1, 1)
+        finish(0)
+        begin(1, 0)
+        relay(1, 1, 1)
+        sends_done()
+        finish(1, 0)
+        begin(1, 1)
+        finish(1, 1)
+        mix(0)
+
+    def inner_order():
+        send_half(1, 0, 1)
+        z_sends((4, 5))
+        enter(2)
+        spread(0, 2)
+        relay(0, 2)
+        near(0, 2)
+        enter(3)
+        send_first(0, 3)
+        units(2, "near")
+        distant(0, 2)
+        produce(2, "far")
+        enter_next(0)
+        units(1, "own")
         loads[2].wait()
-        begin("early")
-        finish("early")
-        relay(0, 3)
-        relay(1, 0)
+        take(1, 0)
+        begin(0)
+        relay(1, 2)
+        send_rest(0, 3)
+        begin(2)
+        finish(2)
+        enter_far()
+        units(3, "own_last")
+        hand(1, 0)
         near(0, 3)
-        units(3, 0, None, 1, 0)
-        distant(0, 3)
-        produce(3, None, 1)
-        enter_next()
-        produce(1)
-        relay(1, 3)
-        begin("late")
-        finish("late")
-        relay(1, 1)
-        begin(1)
-        finish(1)
-        begin(0)
+        produce(3, "side_last", 0)
+        send_first(1, 3, 1)
+        relay(1, 3, 0)
+        send_rest(1, 3, 1)
+        enter_next(1)
+        units(1, "side")
+        relay(1, 3, 1)
+        spread(1, 1, 0)
+        send_first(1, 1, 1)
+        begin(3, 0)
+        finish(3, 0)
+        begin(3, 1)
+        finish(3, 1)
+        relay(1, 1, 0)
+        send_rest(1, 1, 1)
         finish(0)
-
-    def inner_order():
-        enter(3)
-        relay(0, 3)
-        near(0, 3)
-        spread_half(1, 0, 1)
-        units(3, 0, None, 1, 0)
-        distant(0, 3)
-        produce(3, None, 1)
-        relay(1, 3)
-        enter(2)
-        loads[2].wait()
-        begin("early")
-        finish("early")
-        relay(0, 2)
-        relay(1, 0)
-        near(0, 2)
-        units(2, 0, None, 1, 0)
-        distant(0, 2)
-        produce(2, None, 1)
-        enter_next()
-        produce(1)
-        relay(1, 2)
-        begin("late")
-        finish("late")
-        relay(1, 1)
-        begin(1)
-        finish(1)
-        begin(0)
-        finish(0)
+        begin(1, 0)
+        relay(1, 1, 1)
+        sends_done()
+        finish(1, 0)
+        begin(1, 1)
+        finish(1, 1)
+        mix(0)
 
     pl.when(inner == 0)(outer_order)
     pl.when(inner == 1)(inner_order)
 
-    place = lax.broadcasted_iota(jnp.int32, (n_ep * slots, tok_rows), 0).astype(jnp.float32)
-    share = None
-    for k in range(2):
-        spot = (
-            ids_row[k : k + 1, :].astype(jnp.float32) * slots
-            + slot_row[k]
-            + (lead * core).astype(jnp.float32)
-        )
-        part = jnp.where(place == spot, route_row_ref[k : k + 1, :], 0.0)
-        share = part if share is None else share + part
-    share = jnp.transpose(share)
-    share_high = share.astype(jnp.bfloat16)
-    share_low = (share - share_high.astype(jnp.float32)).astype(jnp.bfloat16)
-
-    with jax.named_scope("w_sends"):
-        for box in range(6):
-            for c in range(2):
-                z_copy(box, c).wait_send()
-        pair_copy(core).wait_send()
-        for k in range(pairs):
-            for b in range(2):
-                if b == 0 and k < 2:
-                    continue
-                for d in range(2):
-                    for r in far_parts if k > 1 else whole:
-                        for half in range(2):
-                            block_copy(b, k, d, half, r).wait_send()
-                        relay_copy(b, k, d, r).wait_send()
-        for at in range(PIECES):
-            partner_copy(at).wait_send()
-            for name in (1, "early", "late"):
-                for c in range(2):
-                    back_copy(name, c, at).wait_send()
-
-    with jax.named_scope("w_back"):
-        for at in range(PIECES):
-            for flips in range(1, n_ep):
-                back_arrival(flips, at).wait_recv()
-
-    def mix(i, carry):
-        where = pl.ds(pl.multiple_of(i * COLUMN_TILE, COLUMN_TILE), COLUMN_TILE)
-        table = back[:, :, where].reshape(n_ep * slots, COLUMN_TILE)
-        total = jnp.dot(share_high, table, preferred_element_type=jnp.float32)
-        total = total + jnp.dot(share_low, table, preferred_element_type=jnp.float32)
-        out_ref[:, where] = total.astype(jnp.bfloat16)
-        return carry
-
-    with jax.named_scope("mix"):
-        lax.fori_loop(0, outs // COLUMN_TILE, mix, 0)
+    with jax.named_scope("w_sends_2"):
+        bytes_of(boxes[1].at[1, pl.ds(0, 3)], g_send.at[1, 1], g_recv.at[0, 0]).wait_send()
+        bytes_of(back.at[pl.ds(0, n_ep - 1)], b_send, b_recv.at[0]).wait_send()
+    mix(1)
 
 
 def fused_path(
@@ -672,25 +709,26 @@
             pltpu.VMEM(down_weight.shape[1:], jnp.bfloat16),
             pltpu.VMEM((tok_rows, 128), jnp.float32),
             pltpu.VMEM((tok_rows, width), jnp.bfloat16),
-            pltpu.VMEM((pairs + 2, 2, slots, cols), jnp.bfloat16),
+            pltpu.VMEM((pairs + 3, 2, slots, cols), jnp.bfloat16),
             pltpu.VMEM((n_tp, slots, cols), jnp.bfloat16),
-            pltpu.VMEM((pairs + 2, 2, slots, cols), jnp.bfloat16),
+            pltpu.VMEM((pairs + 3, 2, slots, cols), jnp.bfloat16),
             pltpu.VMEM((2, n_tp, slots, cols), jnp.bfloat16),
             pltpu.VMEM((pairs, n_tp, rows, cols), jnp.bfloat16),
             pltpu.VMEM((pairs, n_tp, rows, hid), jnp.bfloat16),
             pltpu.VMEM((pairs, rows, outs), jnp.bfloat16),
             pltpu.VMEM((n_ep, slots, outs), jnp.bfloat16),
-            pltpu.VMEM((3, rows, hid), jnp.float32),
+            pltpu.VMEM((6, rows, hid), jnp.float32),
+            pltpu.VMEM((tok_rows, outs), jnp.float32),
             dma((4,)),
             dma((3,)),
-            dma((pairs + 2, 2)),
-            dma((pairs + 2, 2)),
+            dma,
+            dma((5,)),
             dma,
             dma,
-            dma((2, pairs, 2, 6)),
-            dma((2, pairs, 2, 6)),
-            dma((pairs, 2, PIECES)),
-            dma((n_ep, PIECES)),
+            dma((2, pairs)),
+            dma((2 + 2 * pairs, 4)),
+            dma,
+            dma((2,)),
         ],
         compiler_params=pltpu.CompilerParams(
             collective_id=0, has_side_effects=True, vmem_limit_bytes=VMEM_BYTES

time: 82.1 us -> 69.9 us (0.85)
  Pallas kernels: 81.2 us -> 69 us
    pallas_call x1, Pallas kernels: 81.2 us -> 69 us  [fused_path(): pl.pallas_call(functools.partial(fused_kernel, n_ep, n_tp, capacity, slot...]
where the time goes in v2:
time: 69.9 us; the launch traced here: 69.8 us
  Pallas kernels  69 us (99%)
  local copies, waits for them, and re-layouts  0.75 us (1%)
    pallas_call x1, Pallas kernels, fused_path(): pl.pallas_call(functools.partial(fused_kernel, n_ep, n_tp, capacity, slot...  69 us

profile of v2, /device:TPU:1, one launch (start us, length us, event | category | flops | bytes accessed | tf_op | source)
XLA Modules:
  0.0 69.8 jit_solution(3851762902256820712)
XLA Ops:
  0.0 69.0 %shard_map.73 = bf16[192,1024]{1,0:T(8,128)(2,1)S(1)} custom-call(bf16[192,4096]{1,0:T(8,128)(2,1)} %tokens_hbm.1, s32[2,192]{1,0:T(2,128)} %bitcast.4, f32[2,192]{1,0:T(2,128)} %bitcast.5, f32[1,4096]{1,0:T(1,128)} %bitcast.3, bf16[1,4096,1024]{2,1,0:T(8,128)(2,1)} %gate_hbm.1, bf16[1,4096,1024]{2,1,0:T(8,128)(2,1)} %up_hbm.1, bf16[1,4096,1024]{2,1,0:T(8,128)(2,1)} %down_hbm.1), custom_call_target="tpu_custom_call" | custom-call | tf_op jit(solution)/shard_map/pallas_call | solution.py:697
  69.0 0.7 %copy.9 = bf16[192,1024]{1,0:T(8,128)(2,1)} copy(bf16[192,1024]{1,0:T(8,128)(2,1)S(1)} %shard_map.73) | data formatting | bytes 786432

commit v3 on v2

--- a/solution.py
+++ b/solution.py
@@ -114,13 +114,17 @@
     scales,
     normed,
     outbox,
+    outedge,
     fullbox,
-    zbox,
-    zfull,
+    fulledge,
+    zedge,
+    pairedge,
     xbuf,
     hbuf,
     obuf,
+    obedge,
     back,
+    backedge,
     acc,
     mixed,
     small_sem,
@@ -151,11 +155,13 @@
     inner = lax.rem(pair + lax.div(pair, jnp.int32(2)), jnp.int32(2))
     chip_of = [flip(pair, k) for k in range(pairs)]
 
+    top, low = pl.ds(0, tok_rows // 2), pl.ds(tok_rows // 2, tok_rows // 2)
     small = (
-        (tokens_hbm, tokens_ref),
         (ids_row_hbm, ids_row_ref),
+        (gain_hbm, gain_ref),
+        (tokens_hbm.at[top], tokens_ref.at[top]),
+        (tokens_hbm.at[low], tokens_ref.at[low]),
         (route_row_hbm, route_row_ref),
-        (gain_hbm, gain_ref),
     )
     small_loads = [
         pltpu.make_async_copy(a, b, small_sem.at[i]) for i, (a, b) in enumerate(small)
@@ -177,12 +183,6 @@
             barrier, inc=1, device_id=(ep, other), device_id_type=pl.DeviceIdType.MESH
         )
 
-    with jax.named_scope("small_wait"):
-        for load in small_loads:
-            load.wait()
-    for load in loads:
-        load.start()
-
     own_cols = pl.ds(pl.multiple_of(tp * cols, cols), cols)
     far_cols = pl.ds(pl.multiple_of(far * cols, cols), cols)
 
@@ -196,8 +196,8 @@
             normed[at, where] = (values * scale * gain_ref[:, where]).astype(jnp.bfloat16)
         return carry
 
-    with jax.named_scope("scale_rows"):
-        lax.fori_loop(0, tok_rows // 32, scale_rows, 0)
+    with jax.named_scope("small_wait"):
+        small_loads[0].wait()
 
     ids_row = ids_row_ref[...]
     expert_col = lax.broadcasted_iota(jnp.int32, (n_ep, tok_rows), 0)
@@ -212,9 +212,19 @@
         jnp.sum(jnp.where(ids_row[k : k + 1, :] == expert_col, before_row, 0.0), axis=0, keepdims=True)
         for k in range(2)
     ]
-    slot_at = (
-        lax.broadcasted_iota(jnp.int32, (slots, tok_rows), 0) - lead * core
-    ).astype(jnp.float32)
+    block_row = lax.broadcasted_iota(jnp.int32, (slots, tok_rows), 0)
+    edge_slot = second * (1 - core) - second
+
+    def slots_at(shift):
+        edge_row = block_row - shift
+        at = jnp.where(
+            block_row < second,
+            block_row + lead * core,
+            jnp.where((edge_row >= second) & (edge_row < capacity), edge_row + edge_slot, -1),
+        )
+        return at.astype(jnp.float32)
+
+    slot_at = slots_at(0)
 
     def pick_of(expert):
         taken = ((ids_row[0:1, :] == expert) & (slot_row[0] == slot_at)) | (
@@ -223,27 +233,43 @@
         return taken.astype(jnp.float32).astype(jnp.bfloat16)
 
     def picked(pick, where):
-        return jnp.dot(pick, normed[:, where], preferred_element_type=jnp.float32).astype(
-            jnp.bfloat16
-        )
-
-    with jax.named_scope("barrier"):
-        pl.semaphore_wait(barrier, n_ep - 1 + 2)
+        return jnp.dot(pick, normed[:, where], preferred_element_type=jnp.float32)
+
+    with jax.named_scope("wait_top"):
+        small_loads[1].wait()
+        small_loads[2].wait()
+    steps = tok_rows // 64
+    with jax.named_scope("scale_top"):
+        lax.fori_loop(0, steps, scale_rows, 0)
+    with jax.named_scope("wait_low"):
+        small_loads[3].wait()
+        small_loads[4].wait()
+    for load in loads:
+        load.start()
+    with jax.named_scope("scale_low"):
+        lax.fori_loop(steps, 2 * steps, scale_rows, 0)
 
     box_cols = (tp, tp, tp, far) + side + (far,)
 
     def box_flip(box):
         return {0: 2, 1: 3, 6: 3}.get(box, 1)
 
-    def z_copy(box, c):
-        return pltpu.make_async_remote_copy(
-            src_ref=outbox.at[box, c],
-            dst_ref=zbox.at[box, core],
-            send_sem=z_send,
-            recv_sem=z_recv.at[(0, 1, 2, 2, 3, 3, 4)[box]],
-            device_id=(flip(pair, box_flip(box)) * 2 + c, tp),
-            device_id_type=pl.DeviceIdType.MESH,
-        )
+    def mains(at):
+        return pl.ds(pl.multiple_of(slots * at, 8), second)
+
+    def z_copies(box, c):
+        for src, dst in (
+            (outbox.at[box, c], xbuf.at[box_flip(box), box_cols[box], mains(core)]),
+            (outedge.at[box, c], zedge.at[box, core]),
+        ):
+            yield pltpu.make_async_remote_copy(
+                src_ref=src,
+                dst_ref=dst,
+                send_sem=z_send.at[box // 4],
+                recv_sem=z_recv.at[(0, 1, 2, 2, 3, 5, 4)[box]],
+                device_id=(flip(pair, box_flip(box)) * 2 + c, tp),
+                device_id_type=pl.DeviceIdType.MESH,
+            )
 
     def bytes_of(ref, send, recv):
         return pltpu.make_async_remote_copy(
@@ -256,19 +282,41 @@
         )
 
     def z_wait(at, ref):
-        bytes_of(ref, z_send, z_recv.at[at]).wait_recv()
+        bytes_of(ref, z_send.at[0], z_recv.at[at]).wait_recv()
+
+    def fold(values):
+        return jnp.concatenate([values[:, : cols // 2], values[:, cols // 2 :]], axis=0)
+
+    def z_fill(box):
+        where = pl.ds(pl.multiple_of(box_cols[box] * cols, cols), cols)
+        for c in range(2):
+            values = picked(pick_of(flip(pair, box_flip(box)) * 2 + c), where)
+            outbox[box, c] = values[:second].astype(jnp.bfloat16)
+            outedge[box, c] = fold(values[second:capacity]).astype(jnp.bfloat16)
+
+    def z_start(box):
+        for c in range(2):
+            for copy in z_copies(box, c):
+                copy.start()
 
     def z_sends(boxes_in_order):
         for box in boxes_in_order:
-            where = pl.ds(pl.multiple_of(box_cols[box] * cols, cols), cols)
-            for c in range(2):
-                pick = pick_of(flip(pair, box_flip(box)) * 2 + c)
-                outbox[box, c] = picked(pick, where)
-                z_copy(box, c).start()
+            z_fill(box)
+            z_start(box)
+
+    def z_first(boxes_in_order):
+        z_start(boxes_in_order[0])
+        z_sends(boxes_in_order[1:])
+
+    pl.when(inner == 1)(lambda: z_fill(0))
+    pl.when(inner == 0)(lambda: z_fill(2))
+    with jax.named_scope("barrier"):
+        pl.semaphore_wait(barrier, n_ep - 1 + 2)
+
 
     with jax.named_scope("z_sends"):
-        pl.when(inner == 1)(lambda: z_sends((0, 1, 2)))
-        pl.when(inner == 0)(lambda: z_sends((2, 0, 3, 1)))
+        pl.when(inner == 1)(lambda: z_first((0, 1, 2)))
+        pl.when(inner == 0)(lambda: z_first((2, 0, 3, 1)))
 
     def norm_rest(i, carry):
         at = pl.ds(pl.multiple_of(i * 32, 32), 32)
@@ -285,31 +333,39 @@
 
     partner = flip(ep, 1)
 
-    def pair_copy(at):
-        return pltpu.make_async_remote_copy(
-            src_ref=fullbox,
-            dst_ref=zfull.at[at],
-            send_sem=pair_send,
-            recv_sem=pair_recv,
-            device_id=(partner, tp),
-            device_id_type=pl.DeviceIdType.MESH,
-        )
+    def pair_copies():
+        for src, dst in (
+            (fullbox, xbuf.at[0, :, mains(core)]),
+            (fulledge, pairedge.at[core]),
+        ):
+            yield pltpu.make_async_remote_copy(
+                src_ref=src,
+                dst_ref=dst,
+                send_sem=pair_send,
+                recv_sem=pair_recv,
+                device_id=(partner, tp),
+                device_id_type=pl.DeviceIdType.MESH,
+            )
 
     with jax.named_scope("pair_pick"):
         theirs = pick_of(partner)
         for j in range(n_tp):
-            fullbox[j] = picked(theirs, slice(j * cols, (j + 1) * cols))
-        pair_copy(core).start()
+            values = picked(theirs, slice(j * cols, (j + 1) * cols))
+            fullbox[j] = values[:second].astype(jnp.bfloat16)
+            fulledge[j] = fold(values[second:capacity]).astype(jnp.bfloat16)
+        for copy in pair_copies():
+            copy.start()
         mine = pick_of(ep)
         for j in range(n_tp):
-            zfull[core, j] = picked(mine, slice(j * cols, (j + 1) * cols))
-
-    edge = slots - second
+            values = picked(mine, slice(j * cols, (j + 1) * cols))
+            xbuf[0, j, mains(core), :] = values[:second].astype(jnp.bfloat16)
+            pairedge[core, j] = fold(values[second:capacity]).astype(jnp.bfloat16)
 
     def join(k, j, low, high):
-        xbuf[k, j, 0:second, :] = low[0:second, :]
-        xbuf[k, j, second:slots, :] = low[second:slots, :] + high[0:edge, :]
-        xbuf[k, j, slots:rows, :] = high[edge:slots, :]
+        for half in range(2):
+            mid = [v[lead * half : lead * half + lead, :] for v in (low, high)]
+            lanes = slice(half * (cols // 2), (half + 1) * (cols // 2))
+            xbuf[k, j, second:slots, lanes] = jnp.concatenate(mid, axis=0)
 
     boxes = (xbuf, hbuf)
     half_cols = cols // 2
@@ -332,7 +388,7 @@
         )
 
     def block_copy(b, k, d, half, r):
-        return g_copy(b, k, tp, half, r, side[d], d if half == d and (b, k) != (0, 3) else 2)
+        return g_copy(b, k, tp, half, r, side[d], d if half == d else 2)
 
     def take(b, k, r=None):
         for d in range(2):
@@ -372,10 +428,7 @@
 
     def near(b, k, r=None):
         with jax.named_scope(f"w_near_{b}_{r}"):
-            if (b, k) == (0, 3):
-                bytes_of(xbuf.at[k, pl.ds(0, 2)], g_send.at[b, k], g_recv.at[1, 2]).wait_recv()
-            else:
-                arrive(b, k, r, 2)
+            arrive(b, k, r, 2)
 
     def distant(b, k, r=None):
         with jax.named_scope(f"w_far_{b}_{r}"):
@@ -383,35 +436,40 @@
 
     def enter(k):
         with jax.named_scope("w_z"):
-            z_wait(k - 2, zbox.at[k - 2])
-        join(k, tp, zbox[k - 2, 0], zbox[k - 2, 1])
+            z_wait(k - 2, xbuf.at[k, tp])
+        join(k, tp, zedge[k - 2, 0], zedge[k - 2, 1])
 
     def enter_far():
         with jax.named_scope("w_zfar"):
-            z_wait(4, zbox.at[6])
-        join(3, far, zbox[6, 0], zbox[6, 1])
+            z_wait(4, xbuf.at[3, far])
+        join(3, far, zedge[6, 0], zedge[6, 1])
 
     def enter_next(part):
+        first_box, count, at = ((2, 2, 2), (4, 1, 3), (5, 1, 5))[part]
         with jax.named_scope(f"w_z1_{part}"):
-            z_wait(2 + part, zbox.at[pl.ds(2 + 2 * part, 2)])
-        for box in range(2 + 2 * part, 4 + 2 * part):
-            join(1, box_cols[box], zbox[box, 0], zbox[box, 1])
+            z_wait(at, xbuf.at[1, pl.ds(0, count)])
+        for box in range(first_box, first_box + count):
+            join(1, box_cols[box], zedge[box, 0], zedge[box, 1])
 
     def dot_blocks(box, k, r, weight, where, blocks):
         depth = box.shape[-1]
         start, stop = spans[r]
         total = None
-        for j in blocks:
+        for j, half in blocks:
+            size = depth if half is None else depth // 2
             at = j * depth if isinstance(j, int) else pl.multiple_of(j * depth, depth)
+            at = at + (half or 0) * size
+            lanes = slice((half or 0) * size, (half or 0) * size + size)
             part = jnp.dot(
-                box[k, j, start:stop, :], weight[pl.ds(at, depth), where],
+                box[k, j, start:stop, lanes], weight[pl.ds(at, size), where],
                 preferred_element_type=jnp.float32,
             )
             total = part if total is None else total + part
         return total
 
-    every = tuple(range(n_tp))
-    close = (tp,) + side
+    every = tuple((j, None) for j in range(n_tp))
+    sides = tuple((j, None) for j in side)
+    close = ((tp, None),) + sides
 
     def column(i):
         return pl.ds(pl.multiple_of(i * COLUMN_TILE, COLUMN_TILE), COLUMN_TILE)
@@ -419,11 +477,14 @@
     stages = {
         None: (every, None, None),
         "near": (close, None, 0),
-        "far": ((far,), 0, None),
-        "own": ((tp, far), None, 2),
-        "side": (side, 2, None),
-        "own_last": ((tp, far), None, 0),
-        "side_last": (side, 0, None),
+        "far": (((far, None),), 0, None),
+        "own": (((tp, None), (far, None)), None, 2),
+        "third": (sides[:1], 2, 2),
+        "fourth": (sides[1:], 2, None),
+        "mine": (close[:1], None, 0),
+        "sides": (sides, 0, 0),
+        "own_last": (((tp, None), (far, None), (side[0], 0), (side[1], 1)), None, 0),
+        "side_last": (((side[0], 1), (side[1], 0)), 0, None),
     }
 
     def units(k, stage=None, halves=both):
@@ -455,32 +516,36 @@
 
     piece = outs // PIECES
 
-    def piece_of(ref, at):
-        return ref.at[:, pl.ds(at * piece, piece)]
-
-    def back_send(k, start, to, at, group_at):
+    def back_copy(src, dst, to, group_at):
         return pltpu.make_async_remote_copy(
-            src_ref=obuf.at[k, pl.ds(start, slots), pl.ds(at * piece, piece)],
-            dst_ref=back.at[ep, :, pl.ds(at * piece, piece)],
-            send_sem=b_send,
+            src_ref=src,
+            dst_ref=dst,
+            send_sem=b_send.at[group_at // 2],
             recv_sem=b_recv.at[group_at],
             device_id=(to, tp),
             device_id_type=pl.DeviceIdType.MESH,
         )
 
+    def back_send(k, c, to, at, group_at):
+        lanes = pl.ds(at * piece, piece)
+        back_copy(obuf.at[k, mains(c), lanes], back.at[ep, :, lanes], to, group_at).start()
+        if at == PIECES - 1:
+            back_copy(obedge.at[k, c], backedge.at[ep], to, group_at).start()
+
     def results(name, stage, r=None):
         k = name
         start, stop = spans[r]
-        blocks, _, keep = stages[stage]
-        at_acc = 5 if name == 0 else 4
+        blocks, begun, keep = stages[stage]
+        at_acc = {0: 5, 1: 2}.get(name, 4)
 
         def tile(i, carry):
             where = column(i)
             total = dot_blocks(hbuf, k, r, down_v, where, blocks)
+            if begun is not None:
+                total = total + acc[at_acc, start:stop, where]
             if keep is not None:
                 acc[at_acc, start:stop, where] = total
                 return carry
-            total = total + acc[at_acc, start:stop, where]
             obuf[k, start:stop, where] = total.astype(jnp.bfloat16)
             return carry
 
@@ -490,17 +555,22 @@
                 lax.fori_loop(at * tiles, (at + 1) * tiles, tile, 0)
             if keep is not None:
                 continue
+            if at == PIECES - 1 and r != 1:
+                mid = obuf[k, second:slots, :].astype(jnp.float32)
+                for c in both:
+                    obedge[k, c] = fold(mid[lead * c : lead * c + lead]).astype(jnp.bfloat16)
             if name == 0:
-                back_send(0, pl.multiple_of(second * (1 - core), 8), partner, at, 0).start()
+                back_send(0, 1 - core, partner, at, 2)
             else:
                 for c in both if r is None else (r,):
-                    back_send(k, second * c, chip_of[name] * 2 + c, at, int(name == 1)).start()
+                    back_send(k, c, chip_of[name] * 2 + c, at, int(name == 1))
         if name == 0 and keep is None:
-            back[ep] = obuf[0, pl.ds(pl.multiple_of(second * core, 8), slots), :]
+            back[ep] = obuf[0, mains(core), :]
+            backedge[ep] = obedge[0, core]
 
     def begin(name, r=None):
         near(1, name, r)
-        results(name, "near", r)
+        results(name, "near" if r is None else "sides", r)
 
     def finish(name, r=None):
         distant(1, name, r)
@@ -508,14 +578,13 @@
 
     mixed_chips = ((pair, chip_of[2], chip_of[3]), (chip_of[1],))
 
-    def share_of(part):
-        place = lax.broadcasted_iota(jnp.int32, (slots, tok_rows), 0)
+    def share_of(part, at_slots):
         shares = []
         for chip in mixed_chips[part]:
             for c in both:
                 share = None
                 for k in range(2):
-                    hit = (ids_row[k : k + 1, :] == chip * 2 + c) & (slot_row[k] == slot_at)
+                    hit = (ids_row[k : k + 1, :] == chip * 2 + c) & (slot_row[k] == at_slots)
                     one = jnp.where(hit, route_row_ref[k : k + 1, :], 0.0)
                     share = one if share is None else share + one
                 shares.append(share)
@@ -525,29 +594,36 @@
         return jnp.concatenate([high, low], axis=1)
 
     def mix(part):
-        share = share_of(part)
+        shares = [share_of(part, at_slots) for at_slots in (slot_at, slots_at(lead))]
         with jax.named_scope(f"w_back_{part}"):
-            got = back.at[pl.ds(0, 2 if part else 5)]
-            bytes_of(got, b_send, b_recv.at[part]).wait_recv()
-
-        def tile(i, carry):
-            where = column(i)
-            blocks = [back[chip * 2 + c, :, where] for chip in mixed_chips[part] for c in both]
-            table = jnp.concatenate(blocks + blocks, axis=0)
-            total = jnp.dot(share, table, preferred_element_type=jnp.float32)
             if part == 0:
-                mixed[:, where] = total
-            else:
-                out_ref[:, where] = (mixed[:, where] + total).astype(jnp.bfloat16)
-            return carry
-
+                half = obuf.at[0, :, pl.ds(0, outs // 2)]
+                bytes_of(half, b_send.at[1], b_recv.at[2]).wait_recv()
+            got = xbuf.at[0, pl.ds(0, 1 if part else 2)]
+            bytes_of(got, b_send.at[0], b_recv.at[part]).wait_recv()
         with jax.named_scope(f"mix_{part}"):
-            lax.fori_loop(0, outs // COLUMN_TILE, tile, 0, unroll=True)
+            for i in range(outs // COLUMN_TILE):
+                where = slice(i * COLUMN_TILE, (i + 1) * COLUMN_TILE)
+                half = i * COLUMN_TILE // (outs // 2)
+                lanes = slice(where.start - half * (outs // 2), where.stop - half * (outs // 2))
+                blocks = []
+                for chip in mixed_chips[part]:
+                    for c in both:
+                        blocks += [back[chip * 2 + c, :, where], backedge[chip * 2 + c, :, lanes]]
+                table = jnp.concatenate(blocks + blocks, axis=0)
+                total = jnp.dot(shares[half], table, preferred_element_type=jnp.float32)
+                if part == 0:
+                    mixed[:, where] = total
+                else:
+                    out_ref[:, where] = (mixed[:, where] + total).astype(jnp.bfloat16)
 
     def sends_done():
         with jax.named_scope("w_sends"):
-            bytes_of(outbox, z_send, z_recv.at[0]).wait_send()
-            pair_copy(core).wait_send()
+            bytes_of(xbuf.at[0], z_send.at[0], z_recv.at[0]).wait_send()
+            bytes_of(xbuf.at[0, pl.ds(0, 3)], z_send.at[1], z_recv.at[0]).wait_send()
+            bytes_of(xbuf.at[0, pl.ds(0, 2)], pair_send, z_recv.at[0]).wait_send()
+            half = obuf.at[0, :, pl.ds(0, outs // 2)]
+            bytes_of(half, b_send.at[1], b_recv.at[2]).wait_send()
             for b in range(2):
                 for k in range(2 - 2 * b, pairs):
                     if (b, k) != (1, 1):
@@ -555,9 +631,9 @@
                         bytes_of(sent, g_send.at[b, k], g_recv.at[0, 0]).wait_send()
 
     with jax.named_scope("w_pair"):
-        pair_copy(1 - core).wait_recv()
+        bytes_of(xbuf.at[0, pl.ds(0, 2)], pair_send, pair_recv).wait_recv()
     for j in range(n_tp):
-        join(0, j, zfull[0, j], zfull[1, j])
+        join(0, j, pairedge[0, j], pairedge[1, j])
     with jax.named_scope("w_gateup"):
         loads[0].wait()
         loads[1].wait()
@@ -586,28 +662,32 @@
         spread(0, 3)
         begin(2)
         finish(2)
+        hand(1, 0)
         enter_far()
+        take(0, 3)
         units(3, "own_last")
-        hand(1, 0)
         near(0, 3)
         produce(3, "side_last", 0)
         send_first(1, 3, 1)
+        finish(0)
+        results(3, "mine")
         relay(1, 3, 0)
         send_rest(1, 3, 1)
         enter_next(1)
-        units(1, "side")
+        units(1, "third")
         relay(1, 3, 1)
-        spread(1, 1, 0)
+        enter_next(2)
+        produce(1, "fourth", 0)
         send_first(1, 1, 1)
         begin(3, 0)
         finish(3, 0)
         begin(3, 1)
-        finish(3, 1)
         relay(1, 1, 0)
         send_rest(1, 1, 1)
-        finish(0)
+        finish(3, 1)
+        results(1, "mine")
+        relay(1, 1, 1)
         begin(1, 0)
-        relay(1, 1, 1)
         sends_done()
         finish(1, 0)
         begin(1, 1)
@@ -635,28 +715,32 @@
         send_rest(0, 3)
         begin(2)
         finish(2)
+        hand(1, 0)
         enter_far()
+        take(0, 3)
         units(3, "own_last")
-        hand(1, 0)
         near(0, 3)
         produce(3, "side_last", 0)
         send_first(1, 3, 1)
+        finish(0)
+        results(3, "mine")
         relay(1, 3, 0)
         send_rest(1, 3, 1)
         enter_next(1)
-        units(1, "side")
+        units(1, "third")
         relay(1, 3, 1)
-        spread(1, 1, 0)
+        enter_next(2)
+        produce(1, "fourth", 0)
         send_first(1, 1, 1)
         begin(3, 0)
         finish(3, 0)
         begin(3, 1)
-        finish(3, 1)
         relay(1, 1, 0)
         send_rest(1, 1, 1)
-        finish(0)
+        finish(3, 1)
+        results(1, "mine")
+        relay(1, 1, 1)
         begin(1, 0)
-        relay(1, 1, 1)
         sends_done()
         finish(1, 0)
         begin(1, 1)
@@ -668,7 +752,7 @@
 
     with jax.named_scope("w_sends_2"):
         bytes_of(boxes[1].at[1, pl.ds(0, 3)], g_send.at[1, 1], g_recv.at[0, 0]).wait_send()
-        bytes_of(back.at[pl.ds(0, n_ep - 1)], b_send, b_recv.at[0]).wait_send()
+        bytes_of(xbuf.at[0, pl.ds(0, 3)], b_send.at[0], b_recv.at[0]).wait_send()
     mix(1)
 
 
@@ -678,6 +762,7 @@
     tok_rows, width = tokens.shape
     capacity, slots = slots_of(n_ep, tokens.shape, expert_ids.shape)
     rows = 2 * capacity
+    main, edge = rows - slots, 2 * (slots - capacity)
     hid = gate_weight.shape[2]
     outs = down_weight.shape[2]
     cols = width // n_tp
@@ -709,26 +794,30 @@
             pltpu.VMEM(down_weight.shape[1:], jnp.bfloat16),
             pltpu.VMEM((tok_rows, 128), jnp.float32),
             pltpu.VMEM((tok_rows, width), jnp.bfloat16),
-            pltpu.VMEM((pairs + 3, 2, slots, cols), jnp.bfloat16),
-            pltpu.VMEM((n_tp, slots, cols), jnp.bfloat16),
-            pltpu.VMEM((pairs + 3, 2, slots, cols), jnp.bfloat16),
-            pltpu.VMEM((2, n_tp, slots, cols), jnp.bfloat16),
+            pltpu.VMEM((pairs + 3, 2, main, cols), jnp.bfloat16),
+            pltpu.VMEM((pairs + 3, 2, edge, cols // 2), jnp.bfloat16),
+            pltpu.VMEM((n_tp, main, cols), jnp.bfloat16),
+            pltpu.VMEM((n_tp, edge, cols // 2), jnp.bfloat16),
+            pltpu.VMEM((pairs + 3, 2, edge, cols // 2), jnp.bfloat16),
+            pltpu.VMEM((2, n_tp, edge, cols // 2), jnp.bfloat16),
             pltpu.VMEM((pairs, n_tp, rows, cols), jnp.bfloat16),
             pltpu.VMEM((pairs, n_tp, rows, hid), jnp.bfloat16),
             pltpu.VMEM((pairs, rows, outs), jnp.bfloat16),
-            pltpu.VMEM((n_ep, slots, outs), jnp.bfloat16),
+            pltpu.VMEM((pairs, 2, edge, outs // 2), jnp.bfloat16),
+            pltpu.VMEM((n_ep, main, outs), jnp.bfloat16),
+            pltpu.VMEM((n_ep, edge, outs // 2), jnp.bfloat16),
             pltpu.VMEM((6, rows, hid), jnp.float32),
             pltpu.VMEM((tok_rows, outs), jnp.float32),
-            dma((4,)),
+            dma((5,)),
             dma((3,)),
-            dma,
-            dma((5,)),
+            dma((2,)),
+            dma((6,)),
             dma,
             dma,
             dma((2, pairs)),
             dma((2 + 2 * pairs, 4)),
-            dma,
             dma((2,)),
+            dma((3,)),
         ],
         compiler_params=pltpu.CompilerParams(
             collective_id=0, has_side_effects=True, vmem_limit_bytes=VMEM_BYTES
@@ -747,7 +836,9 @@
     args = (tokens, expert_ids, route_weight, norm_gain, gate_weight, up_weight, down_weight)
     fits = n_tp == 4 and n_ep == 8 and gate_weight.shape[0] == 1 and expert_ids.shape[1] == 2
     capacity, slots = slots_of(n_ep, tokens.shape, expert_ids.shape)
-    if fits and capacity % 4 == 0 and slots > capacity:
+    cols = tokens.shape[1] // n_tp
+    even = gate_weight.shape[2] == cols and down_weight.shape[2] == cols
+    if fits and even and capacity % 4 == 0 and slots - capacity == 4:
         return fused_path(n_ep, n_tp, *args)
     return plain_path(*args)
 

time: 69.9 us -> 67.3 us (0.963)
  Pallas kernels: 69 us -> 66.4 us
    pallas_call x1, Pallas kernels: 69 us -> 66.4 us  [fused_path(): pl.pallas_call(functools.partial(fused_kernel, n_ep, n_tp, capacity, slot...]
where the time goes in v3:
time: 67.3 us; the launch traced here: 67.1 us
  Pallas kernels  66.4 us (99%)
  local copies, waits for them, and re-layouts  0.75 us (1%)
    pallas_call x1, Pallas kernels, fused_path(): pl.pallas_call(functools.partial(fused_kernel, n_ep, n_tp, capacity, slot...  66.4 us

profile of v3, /device:TPU:1, one launch (start us, length us, event | category | flops | bytes accessed | tf_op | source)
XLA Modules:
  0.0 67.1 jit_solution(7836626724266126930)
XLA Ops:
  0.0 66.4 %shard_map.73 = bf16[192,1024]{1,0:T(8,128)(2,1)S(1)} custom-call(bf16[192,4096]{1,0:T(8,128)(2,1)} %tokens_hbm.1, s32[2,192]{1,0:T(2,128)} %bitcast.4, f32[2,192]{1,0:T(2,128)} %bitcast.5, f32[1,4096]{1,0:T(1,128)} %bitcast.3, bf16[1,4096,1024]{2,1,0:T(8,128)(2,1)} %gate_hbm.1, bf16[1,4096,1024]{2,1,0:T(8,128)(2,1)} %up_hbm.1, bf16[1,4096,1024]{2,1,0:T(8,128)(2,1)} %down_hbm.1), custom_call_target="tpu_custom_call" | custom-call | tf_op jit(solution)/shard_map/pallas_call | solution.py:782
  66.4 0.7 %copy.9 = bf16[192,1024]{1,0:T(8,128)(2,1)} copy(bf16[192,1024]{1,0:T(8,128)(2,1)S(1)} %shard_map.73) | data formatting | bytes 786432

commit v4 on v3

--- a/solution.py
+++ b/solution.py
@@ -168,10 +168,14 @@
     ]
     for load in small_loads:
         load.start()
-    loads = [
-        pltpu.make_async_copy(hbm.at[0], vmem, weight_sem.at[i])
-        for i, (hbm, vmem) in enumerate(((gate_hbm, gate_v), (up_hbm, up_v), (down_hbm, down_v)))
+    half_hid = hid // 2
+    parts = [
+        (hbm.at[0, :, lanes], vmem.at[:, lanes])
+        for lanes in (pl.ds(0, half_hid), pl.ds(half_hid, half_hid))
+        for hbm, vmem in ((gate_hbm, gate_v), (up_hbm, up_v))
     ]
+    parts.append((down_hbm.at[0], down_v))
+    loads = [pltpu.make_async_copy(a, b, weight_sem.at[i]) for i, (a, b) in enumerate(parts)]
 
     barrier = pltpu.get_barrier_semaphore()
     for k in range(1, n_ep):
@@ -294,8 +298,8 @@
             outbox[box, c] = values[:second].astype(jnp.bfloat16)
             outedge[box, c] = fold(values[second:capacity]).astype(jnp.bfloat16)
 
-    def z_start(box):
-        for c in range(2):
+    def z_start(box, cs=(0, 1)):
+        for c in cs:
             for copy in z_copies(box, c):
                 copy.start()
 
@@ -303,20 +307,6 @@
         for box in boxes_in_order:
             z_fill(box)
             z_start(box)
-
-    def z_first(boxes_in_order):
-        z_start(boxes_in_order[0])
-        z_sends(boxes_in_order[1:])
-
-    pl.when(inner == 1)(lambda: z_fill(0))
-    pl.when(inner == 0)(lambda: z_fill(2))
-    with jax.named_scope("barrier"):
-        pl.semaphore_wait(barrier, n_ep - 1 + 2)
-
-
-    with jax.named_scope("z_sends"):
-        pl.when(inner == 1)(lambda: z_first((0, 1, 2)))
-        pl.when(inner == 0)(lambda: z_first((2, 0, 3, 1)))
 
     def norm_rest(i, carry):
         at = pl.ds(pl.multiple_of(i * 32, 32), 32)
@@ -327,9 +317,6 @@
                 jnp.bfloat16
             )
         return carry
-
-    with jax.named_scope("norm_rest"):
-        lax.fori_loop(0, tok_rows // 32, norm_rest, 0)
 
     partner = flip(ep, 1)
 
@@ -347,12 +334,38 @@
                 device_id_type=pl.DeviceIdType.MESH,
             )
 
-    with jax.named_scope("pair_pick"):
+    def pair_fill():
+        lax.fori_loop(0, tok_rows // 32, norm_rest, 0)
         theirs = pick_of(partner)
         for j in range(n_tp):
             values = picked(theirs, slice(j * cols, (j + 1) * cols))
             fullbox[j] = values[:second].astype(jnp.bfloat16)
             fulledge[j] = fold(values[second:capacity]).astype(jnp.bfloat16)
+
+    def outer_fill():
+        z_fill(2)
+        z_fill(0)
+
+    def outer_sends():
+        for c in range(2):
+            z_start(2, (c,))
+            z_start(0, (c,))
+        pair_fill()
+
+    def inner_sends():
+        z_start(0)
+        z_sends((2,))
+        pair_fill()
+
+    with jax.named_scope("fill"):
+        pl.when(inner == 1)(lambda: z_fill(0))
+        pl.when(inner == 0)(outer_fill)
+    with jax.named_scope("barrier"):
+        pl.semaphore_wait(barrier, n_ep - 1 + 2)
+    with jax.named_scope("z_sends"):
+        pl.when(inner == 1)(inner_sends)
+        pl.when(inner == 0)(outer_sends)
+    with jax.named_scope("pair_pick"):
         for copy in pair_copies():
             copy.start()
         mine = pick_of(ep)
@@ -360,6 +373,8 @@
             values = picked(mine, slice(j * cols, (j + 1) * cols))
             xbuf[0, j, mains(core), :] = values[:second].astype(jnp.bfloat16)
             pairedge[core, j] = fold(values[second:capacity]).astype(jnp.bfloat16)
+        pl.when(inner == 1)(lambda: z_sends((1,)))
+        pl.when(inner == 0)(lambda: z_sends((3, 1)))
 
     def join(k, j, low, high):
         for half in range(2):
@@ -637,9 +652,12 @@
     with jax.named_scope("w_gateup"):
         loads[0].wait()
         loads[1].wait()
-    pl.when(inner == 1)(lambda: z_sends((3, 6)))
     units(0, None, (0,))
     send_half(1, 0, 0)
+    pl.when(inner == 1)(lambda: z_sends((3, 6)))
+    with jax.named_scope("w_gateup"):
+        loads[2].wait()
+        loads[3].wait()
     units(0, None, (1,))
 
     def outer_order():
@@ -654,7 +672,7 @@
         produce(2, "far")
         enter_next(0)
         units(1, "own")
-        loads[2].wait()
+        loads[4].wait()
         take(1, 0)
         begin(0)
         relay(1, 2)
@@ -708,7 +726,7 @@
         produce(2, "far")
         enter_next(0)
         units(1, "own")
-        loads[2].wait()
+        loads[4].wait()
         take(1, 0)
         begin(0)
         relay(1, 2)
@@ -809,7 +827,7 @@
             pltpu.VMEM((6, rows, hid), jnp.float32),
             pltpu.VMEM((tok_rows, outs), jnp.float32),
             dma((5,)),
-            dma((3,)),
+            dma((5,)),
             dma((2,)),
             dma((6,)),
             dma,

time: 67.3 us -> 66.5 us (0.988)
  Pallas kernels: 66.4 us -> 65.6 us
    pallas_call x1, Pallas kernels: 66.4 us -> 65.6 us  [fused_path(): pl.pallas_call(functools.partial(fused_kernel, n_ep, n_tp, capacity, slot...]
where the time goes in v4:
time: 66.5 us; the launch traced here: 66.3 us
  Pallas kernels  65.6 us (99%)
  local copies, waits for them, and re-layouts  0.75 us (1%)
    pallas_call x1, Pallas kernels, fused_path(): pl.pallas_call(functools.partial(fused_kernel, n_ep, n_tp, capacity, slot...  65.6 us

profile of v4, /device:TPU:1, one launch (start us, length us, event | category | flops | bytes accessed | tf_op | source)
XLA Modules:
  0.0 66.3 jit_solution(7222110441782160974)
XLA Ops:
  0.0 65.6 %shard_map.73 = bf16[192,1024]{1,0:T(8,128)(2,1)S(1)} custom-call(bf16[192,4096]{1,0:T(8,128)(2,1)} %tokens_hbm.1, s32[2,192]{1,0:T(2,128)} %bitcast.4, f32[2,192]{1,0:T(2,128)} %bitcast.5, f32[1,4096]{1,0:T(1,128)} %bitcast.3, bf16[1,4096,1024]{2,1,0:T(8,128)(2,1)} %gate_hbm.1, bf16[1,4096,1024]{2,1,0:T(8,128)(2,1)} %up_hbm.1, bf16[1,4096,1024]{2,1,0:T(8,128)(2,1)} %down_hbm.1), custom_call_target="tpu_custom_call" | custom-call | tf_op jit(solution)/shard_map/pallas_call | solution.py:800
  65.6 0.7 %copy.9 = bf16[192,1024]{1,0:T(8,128)(2,1)} copy(bf16[192,1024]{1,0:T(8,128)(2,1)S(1)} %shard_map.73) | data formatting | bytes 786432

commit v5 on v4

--- a/solution.py
+++ b/solution.py
@@ -719,9 +719,9 @@
         spread(0, 2)
         relay(0, 2)
         near(0, 2)
+        units(2, "near")
         enter(3)
         send_first(0, 3)
-        units(2, "near")
         distant(0, 2)
         produce(2, "far")
         enter_next(0)
@@ -746,9 +746,10 @@
         send_rest(1, 3, 1)
         enter_next(1)
         units(1, "third")
+        enter_next(2)
+        units(1, "fourth")
         relay(1, 3, 1)
-        enter_next(2)
-        produce(1, "fourth", 0)
+        spread(1, 1, 0)
         send_first(1, 1, 1)
         begin(3, 0)
         finish(3, 0)

time: 66.5 us -> 66 us (level)
  no operation moved by 1% of the time
where the time goes in v5:
time: 66 us; the launch traced here: 65.9 us
  Pallas kernels  65.1 us (99%)
  local copies, waits for them, and re-layouts  0.75 us (1%)
    pallas_call x1, Pallas kernels, fused_path(): pl.pallas_call(functools.partial(fused_kernel, n_ep, n_tp, capacity, slot...  65.1 us

profile of v5, /device:TPU:1, one launch (start us, length us, event | category | flops | bytes accessed | tf_op | source)
XLA Modules:
  0.0 65.9 jit_solution(7520426867943672276)
XLA Ops:
  0.0 65.1 %shard_map.73 = bf16[192,1024]{1,0:T(8,128)(2,1)S(1)} custom-call(bf16[192,4096]{1,0:T(8,128)(2,1)} %tokens_hbm.1, s32[2,192]{1,0:T(2,128)} %bitcast.4, f32[2,192]{1,0:T(2,128)} %bitcast.5, f32[1,4096]{1,0:T(1,128)} %bitcast.3, bf16[1,4096,1024]{2,1,0:T(8,128)(2,1)} %gate_hbm.1, bf16[1,4096,1024]{2,1,0:T(8,128)(2,1)} %up_hbm.1, bf16[1,4096,1024]{2,1,0:T(8,128)(2,1)} %down_hbm.1), custom_call_target="tpu_custom_call" | custom-call | tf_op jit(solution)/shard_map/pallas_call | solution.py:801
  65.1 0.7 %copy.9 = bf16[192,1024]{1,0:T(8,128)(2,1)} copy(bf16[192,1024]{1,0:T(8,128)(2,1)S(1)} %shard_map.73) | data formatting | bytes 786432
